TPU v7x, 128 devices: a whole 4x4x4 slice. The times are simulated.
128 devices in a mesh: sp: 16 (over z, x), tp: 8 (over y, core).
Axes of the slice: x: 4, y: 4, z: 4, core: 2. Of those that a mesh axis runs over, the one named last changes fastest.
Arguments:
- query_narrow: bfloat16 [4096, 1024], P('sp', 'tp'), may hold values from -6 to 6
- key_narrow: bfloat16 [4096, 1024], P('sp', 'tp'), may hold values from -6 to 6
- value_narrow: bfloat16 [4096, 1024], P('sp', 'tp'), may hold values from -12 to 12
- query_broad: bfloat16 [4096, 1024], P('sp', 'tp'), may hold values from -6 to 6
- key_broad: bfloat16 [4096, 1024], P('sp', 'tp'), may hold values from -6 to 6
- value_broad: bfloat16 [4096, 1024], P('sp', 'tp'), may hold values from -12 to 12
- offset_narrow: bfloat16 [16, 4096], P('tp', 'sp'), as said below
- offset_broad: bfloat16 [8, 4096], P('tp', 'sp'), as said below
- residual: bfloat16 [4096, 2048], P(('sp', 'tp')), may hold values from -6 to 6
- out_narrow: bfloat16 [1024, 2048], P('tp'), may hold values from -0.25 to 0.25
- out_broad: bfloat16 [1024, 2048], P('tp'), may hold values from -0.25 to 0.25
- norm_gain: float32 [2048], replicated, may hold values from 0.1 to 1.9
- up_proj: bfloat16 [2048, 8192], P('sp', 'tp'), may hold values from -0.125 to 0.125
- down_proj: bfloat16 [8192, 2048], P('tp', 'sp'), may hold values from -0.0625 to 0.0625
Outputs:
- output: bfloat16 [4096, 2048], P(('sp', 'tp'))
Inputs may be any that keep to these rules, and one draw needn't show every extreme that they name: `offset_narrow`: additive score offsets of each head for each key position. `offset_broad`: additive score offsets of each head for each key position.
All inputs are finite; a program needn't handle non-finite values.
Results may differ from a plain program's by a relative error of at most 0.018.
Values may be sent and summed in bfloat16 or wider, within the bound.
A program may use at most 64 MiB of HBM per device.

v0:
```python
import math

import jax
import jax.numpy as jnp
from jax import lax
from jax.sharding import PartitionSpec as P

NARROW_SIZE = 64
BROAD_SIZE = 128


def turned_gather(arrays, axis, dims):
    turned = [jnp.moveaxis(a, dim, 0) for a, dim in zip(arrays, dims)]
    widths = [t[0].size for t in turned]
    both = jnp.concatenate([t.reshape(-1, w) for t, w in zip(turned, widths)], axis=1)
    whole = lax.all_gather(both, axis, axis=0, tiled=True)
    tiles = jnp.split(whole, [sum(widths[:k]) for k in range(1, len(widths))], axis=1)
    return tuple(
        (
            jnp.moveaxis(b.reshape(-1, *t.shape[1:]), 0, dim)
            for b, t, dim in zip(tiles, turned, dims)
        )
    )


def cut_along(value, dim, count):
    dims = value.shape
    tiles = value.reshape(*dims[:dim], count, dims[dim] // count, *dims[dim + 1 :])
    return jnp.moveaxis(tiles, dim, 0)


def summed_on_arrival(value, axis, dim):
    count = lax.axis_size(axis)
    tiles = lax.all_to_all(cut_along(value, dim, count), axis, 0, 0, tiled=True)
    return jnp.sum(tiles.astype(jnp.float32), axis=0)


def from_everyone(value, axis):
    copies = jnp.broadcast_to(value, (lax.axis_size(axis), *value.shape))
    return lax.all_to_all(copies, axis, split_axis=0, concat_axis=0, tiled=True)


def in_order(tiles, dim):
    dims = list(tiles.shape[1:])
    dims[dim] *= tiles.shape[0]
    return jnp.moveaxis(tiles, 0, dim).reshape(dims)


def collect(value, axis, dim):
    tiles = from_everyone(value, axis)
    return in_order(tiles, dim)


def on_gathered_pieces(value, axis, dim, work, out_dim):
    width = value.shape[dim]
    pieces = jnp.split(value, 2, axis=dim) if width % 2 == 0 else [value]
    leading = jnp.arange(lax.axis_size(axis)) * width
    tiles = [lax.all_gather(share, axis) for share in pieces]
    made = [jax.vmap(work)(b, leading + k * (width // len(pieces))) for k, b in enumerate(tiles)]
    return in_order(jnp.concatenate(made, axis=out_dim + 1), out_dim)


def stick_block(state, query, keys_block, values_block, offsets, query_pos, key_pos, head_size):
    keep_sum, running = state
    row_count = query.shape[0]
    total_heads = query.shape[1] // head_size
    key_count = keys_block.shape[0]
    q_heads = query.reshape(row_count, total_heads, head_size)
    k_heads = keys_block.reshape(key_count, total_heads, head_size)
    v_heads = values_block.reshape(key_count, total_heads, head_size)
    scores = jnp.einsum(
        "qhe,khe->hqk", q_heads, k_heads, preferred_element_type=jnp.float32
    ) * head_size ** (-0.5)
    scores = scores + offsets.astype(jnp.float32)[:, None, :]
    causal = (key_pos[None, :] < query_pos[:, None])[None]
    log_keep = jnp.where(causal, jax.nn.log_sigmoid(-scores), 0.0)
    keep_after = lax.cumsum(log_keep, axis=2, reverse=True) - log_keep
    weight = jnp.where(
        causal, jnp.exp(jax.nn.log_sigmoid(scores) + keep_after + keep_sum[:, :, None]), 0.0
    )
    weight = weight.astype(jnp.bfloat16)
    running = running + jnp.einsum(
        "hqk,khe->qhe", weight, v_heads, preferred_element_type=jnp.float32
    )
    return (keep_sum + jnp.sum(log_keep, axis=2), running)


def attend_block(states, pieces, query_pos, key_pos, queries):
    key_n, value_n, key_b, value_b, off_n, off_b = pieces
    state_narrow = stick_block(
        states[0], queries[0], key_n, value_n, off_n, query_pos, key_pos, NARROW_SIZE
    )
    state_broad = stick_block(
        states[1], queries[1], key_b, value_b, off_b, query_pos, key_pos, BROAD_SIZE
    )
    return (state_narrow, state_broad)


def local(
    query_narrow,
    key_narrow,
    value_narrow,
    query_broad,
    key_broad,
    value_broad,
    offset_narrow,
    offset_broad,
    residual,
    out_narrow,
    out_broad,
    norm_gain,
    up_proj,
    down_proj,
):
    tok_dev = query_narrow.shape[0]
    my_shard = lax.axis_index("sp")
    query_pos = my_shard * tok_dev + jnp.arange(tok_dev, dtype=jnp.int32)
    queries = (query_narrow, query_broad)

    def empty_state(total_heads, head_size):
        return (
            jnp.zeros((total_heads, tok_dev), jnp.float32),
            jnp.zeros((tok_dev, total_heads, head_size), jnp.float32),
        )

    states = (
        empty_state(offset_narrow.shape[0], NARROW_SIZE),
        empty_state(offset_broad.shape[0], BROAD_SIZE),
    )
    own_keys = (key_narrow, value_narrow, key_broad, value_broad, offset_narrow, offset_broad)
    whole_keys = turned_gather(
        (own_keys[0], own_keys[1], own_keys[2], own_keys[3], own_keys[4], own_keys[5]),
        "sp",
        (0, 0, 0, 0, 1, 1),
    )
    key_span = math.gcd(tok_dev, 512)
    block_count = (my_shard + 1) * (tok_dev // key_span)

    def sweep(turn_index, current):
        first_row = (block_count - 1 - turn_index) * key_span
        row_pieces = tuple(
            (lax.dynamic_slice_in_dim(array, first_row, key_span, 0) for array in whole_keys[:4])
        )
        col_pieces = tuple(
            (lax.dynamic_slice_in_dim(array, first_row, key_span, 1) for array in whole_keys[4:])
        )
        key_pos = first_row + jnp.arange(key_span, dtype=jnp.int32)
        return attend_block(current, row_pieces + col_pieces, query_pos, key_pos, queries)

    states = lax.fori_loop(0, block_count, sweep, states)
    mixed_narrow = states[0][1].reshape(tok_dev, -1).astype(jnp.bfloat16)
    mixed_broad = states[1][1].reshape(tok_dev, -1).astype(jnp.bfloat16)
    attended = summed_on_arrival(
        (
            jnp.dot(mixed_narrow, out_narrow, preferred_element_type=jnp.float32)
            + jnp.dot(mixed_broad, out_broad, preferred_element_type=jnp.float32)
        ).astype(jnp.bfloat16),
        "tp",
        0,
    )
    updated = residual.astype(jnp.float32) + attended
    scale = lax.rsqrt(jnp.mean(updated * updated, axis=-1, keepdims=True) + 1e-06)
    normed = (updated * scale * norm_gain).astype(jnp.bfloat16)
    gathered = collect(normed, "tp", 0)
    pre_act = jnp.dot(
        gathered,
        lax.all_gather(up_proj, "sp", axis=0, tiled=True),
        preferred_element_type=jnp.float32,
    )
    hidden = jnp.square(jax.nn.relu(pre_act)).astype(jnp.bfloat16)

    def project(shard_piece, row_start):
        return jnp.dot(hidden, shard_piece, preferred_element_type=jnp.float32)

    partial_sums = on_gathered_pieces(down_proj, "sp", 1, project, 1)
    channel = summed_on_arrival(partial_sums.astype(jnp.bfloat16), "tp", 0)
    return (updated + channel).astype(jnp.bfloat16)


def solution(mesh):
    return jax.shard_map(
        local,
        mesh=mesh,
        in_specs=(
            P("sp", "tp"),
            P("sp", "tp"),
            P("sp", "tp"),
            P("sp", "tp"),
            P("sp", "tp"),
            P("sp", "tp"),
            P("tp", "sp"),
            P("tp", "sp"),
            P(("sp", "tp"), None),
            P("tp", None),
            P("tp", None),
            P(),
            P("sp", "tp"),
            P("tp", "sp"),
        ),
        out_specs=P(("sp", "tp"), None),
        check_vma=False,
    )
```

profile of v0, /device:TPU:102, one launch (start us, length us, event | category | flops | bytes accessed | tf_op | source)
XLA Modules:
  0.0 342.0 jit_solution(4118133415750312991)
XLA Ops:
  8.2 1.8 concatenate.7
  10.1 1.9 fusion.43
  13.5 52.2 %all-gather.7.cloned.1.call-done = bf16[4096,515]{1,0:T(8,128)(2,1)} async-done(((bf16[256,515]{1,0:T(8,128)(2,1)}), bf16[4096,515]{1,0:T(8,128)(2,1)}) %all-gather.7.cloned.1.call-update) | async-done | bytes 4218896 | tf_op jit(solution)/shard_map/all_gather | solution.py:16
  65.7 1.3 slice_bitcast_fusion.3
  67.3 2.0 slice_reduce_fusion
  69.3 3.9 %fusion.42 = (bf16[4096,128]{1,0:T(8,128)(2,1)S(1)}, bf16[4096,128]{1,0:T(8,128)(2,1)}, bf16[4096,128]{1,0:T(8,128)(2,1)}, bf16[4096,128]{1,0:T(8,128)(2,1)}) fusion(bf16[4096,515]{1,0:T(8,128)(2,1)} %all-gather.7.cloned.1.call-done), kind=kLoop, calls=%fused_computation.76 | loop fusion | bytes 8388608 | tf_op jit(solution)/shard_map/split | solution.py:17
  73.3 191.5 %while.19 = (s32[]{:T(128)}, f32[2,256]{1,0:T(2,128)S(1)}, f32[256,2,64]{0,2,1:T(8,128)S(1)}, f32[1,256]{1,0:T(1,128)S(1)}, f32[256,1,128]{0,2,1:T(8,128)S(1)}, ...) while((s32[]{:T(128)}, f32[2,256]{1,0:T(2,128)S(1)}, ...), condition=%wide.region_7.8_spmd.clone, body=%wide.region_0.7_spmd.clone.sunk | while | flops 98831880 | bytes 9842459 | solution.py:150
  75.1 4.6 %fusion.92 = f32[2,256,2,128]{1,2,3,0:T(2,128)S(1)} fusion(f32[2,256,2,128]{1,3,2,0:T(8,128)S(1)} %bitcast.125), kind=kOutput, calls=%fused_computation.24.clone.1 | output fusion | flops 16646144 | bytes 1048576 | tf_op jit(solution)/shard_map/reduce-window.8
  81.1 1.2 fusion.96
  82.3 2.3 fusion.97
  87.0 4.6 %fusion.92 = f32[2,256,2,128]{1,2,3,0:T(2,128)S(1)} fusion(f32[2,256,2,128]{1,3,2,0:T(8,128)S(1)} %bitcast.125), kind=kOutput, calls=%fused_computation.24.clone.1 | output fusion | flops 16646144 | bytes 1048576 | tf_op jit(solution)/shard_map/reduce-window.8
  93.1 1.2 fusion.96
  94.3 2.3 fusion.97
  99.0 4.6 %fusion.92 = f32[2,256,2,128]{1,2,3,0:T(2,128)S(1)} fusion(f32[2,256,2,128]{1,3,2,0:T(8,128)S(1)} %bitcast.125), kind=kOutput, calls=%fused_computation.24.clone.1 | output fusion | flops 16646144 | bytes 1048576 | tf_op jit(solution)/shard_map/reduce-window.8
  105.0 1.2 fusion.96
  106.2 2.3 fusion.97
  111.0 4.6 %fusion.92 = f32[2,256,2,128]{1,2,3,0:T(2,128)S(1)} fusion(f32[2,256,2,128]{1,3,2,0:T(8,128)S(1)} %bitcast.125), kind=kOutput, calls=%fused_computation.24.clone.1 | output fusion | flops 16646144 | bytes 1048576 | tf_op jit(solution)/shard_map/reduce-window.8
  117.0 1.2 fusion.96
  118.2 2.3 fusion.97
  123.0 4.6 %fusion.92 = f32[2,256,2,128]{1,2,3,0:T(2,128)S(1)} fusion(f32[2,256,2,128]{1,3,2,0:T(8,128)S(1)} %bitcast.125), kind=kOutput, calls=%fused_computation.24.clone.1 | output fusion | flops 16646144 | bytes 1048576 | tf_op jit(solution)/shard_map/reduce-window.8
  129.0 1.2 fusion.96
  130.2 2.3 fusion.97
  134.9 4.6 %fusion.92 = f32[2,256,2,128]{1,2,3,0:T(2,128)S(1)} fusion(f32[2,256,2,128]{1,3,2,0:T(8,128)S(1)} %bitcast.125), kind=kOutput, calls=%fused_computation.24.clone.1 | output fusion | flops 16646144 | bytes 1048576 | tf_op jit(solution)/shard_map/reduce-window.8
  141.0 1.2 fusion.96
  142.2 2.3 fusion.97
  146.9 4.6 %fusion.92 = f32[2,256,2,128]{1,2,3,0:T(2,128)S(1)} fusion(f32[2,256,2,128]{1,3,2,0:T(8,128)S(1)} %bitcast.125), kind=kOutput, calls=%fused_computation.24.clone.1 | output fusion | flops 16646144 | bytes 1048576 | tf_op jit(solution)/shard_map/reduce-window.8
  152.9 1.2 fusion.96
  154.1 2.3 fusion.97
  158.9 4.6 %fusion.92 = f32[2,256,2,128]{1,2,3,0:T(2,128)S(1)} fusion(f32[2,256,2,128]{1,3,2,0:T(8,128)S(1)} %bitcast.125), kind=kOutput, calls=%fused_computation.24.clone.1 | output fusion | flops 16646144 | bytes 1048576 | tf_op jit(solution)/shard_map/reduce-window.8
  164.9 1.2 fusion.96
  166.1 2.3 fusion.97
  170.9 4.6 %fusion.92 = f32[2,256,2,128]{1,2,3,0:T(2,128)S(1)} fusion(f32[2,256,2,128]{1,3,2,0:T(8,128)S(1)} %bitcast.125), kind=kOutput, calls=%fused_computation.24.clone.1 | output fusion | flops 16646144 | bytes 1048576 | tf_op jit(solution)/shard_map/reduce-window.8
  176.9 1.2 fusion.96
  178.1 2.3 fusion.97
  182.8 4.6 %fusion.92 = f32[2,256,2,128]{1,2,3,0:T(2,128)S(1)} fusion(f32[2,256,2,128]{1,3,2,0:T(8,128)S(1)} %bitcast.125), kind=kOutput, calls=%fused_computation.24.clone.1 | output fusion | flops 16646144 | bytes 1048576 | tf_op jit(solution)/shard_map/reduce-window.8
  188.8 1.2 fusion.96
  190.0 2.3 fusion.97
  194.8 4.6 %fusion.92 = f32[2,256,2,128]{1,2,3,0:T(2,128)S(1)} fusion(f32[2,256,2,128]{1,3,2,0:T(8,128)S(1)} %bitcast.125), kind=kOutput, calls=%fused_computation.24.clone.1 | output fusion | flops 16646144 | bytes 1048576 | tf_op jit(solution)/shard_map/reduce-window.8
  200.8 1.2 fusion.96
  202.0 2.3 fusion.97
  206.8 4.6 %fusion.92 = f32[2,256,2,128]{1,2,3,0:T(2,128)S(1)} fusion(f32[2,256,2,128]{1,3,2,0:T(8,128)S(1)} %bitcast.125), kind=kOutput, calls=%fused_computation.24.clone.1 | output fusion | flops 16646144 | bytes 1048576 | tf_op jit(solution)/shard_map/reduce-window.8
  212.8 1.2 fusion.96
  214.0 2.3 fusion.97
  218.7 4.6 %fusion.92 = f32[2,256,2,128]{1,2,3,0:T(2,128)S(1)} fusion(f32[2,256,2,128]{1,3,2,0:T(8,128)S(1)} %bitcast.125), kind=kOutput, calls=%fused_computation.24.clone.1 | output fusion | flops 16646144 | bytes 1048576 | tf_op jit(solution)/shard_map/reduce-window.8
  224.7 1.2 fusion.96
  225.9 2.3 fusion.97
  230.7 4.6 %fusion.92 = f32[2,256,2,128]{1,2,3,0:T(2,128)S(1)} fusion(f32[2,256,2,128]{1,3,2,0:T(8,128)S(1)} %bitcast.125), kind=kOutput, calls=%fused_computation.24.clone.1 | output fusion | flops 16646144 | bytes 1048576 | tf_op jit(solution)/shard_map/reduce-window.8
  236.7 1.2 fusion.96
  237.9 2.3 fusion.97
  242.7 4.6 %fusion.92 = f32[2,256,2,128]{1,2,3,0:T(2,128)S(1)} fusion(f32[2,256,2,128]{1,3,2,0:T(8,128)S(1)} %bitcast.125), kind=kOutput, calls=%fused_computation.24.clone.1 | output fusion | flops 16646144 | bytes 1048576 | tf_op jit(solution)/shard_map/reduce-window.8
  248.7 1.2 fusion.96
  249.9 2.3 fusion.97
  254.6 4.6 %fusion.92 = f32[2,256,2,128]{1,2,3,0:T(2,128)S(1)} fusion(f32[2,256,2,128]{1,3,2,0:T(8,128)S(1)} %bitcast.125), kind=kOutput, calls=%fused_computation.24.clone.1 | output fusion | flops 16646144 | bytes 1048576 | tf_op jit(solution)/shard_map/reduce-window.8
  260.6 1.2 fusion.96
  261.8 2.3 fusion.97
  266.4 20.2 %all_to_all.15 = bf16[8,32,2048]{2,1,0:T(8,128)(2,1)S(1)} all-to-all(bf16[8,32,2048]{2,1,0:T(8,128)(2,1)S(1)} %bitcast.134), channel_id=1, replica_groups=mesh['sp'=16,'tp'=8] {'tp'}, dimensions={0} | all-to-all | bytes 2097152 | tf_op jit(solution)/shard_map/all_to_all | solution.py:34
  287.0 1.1 broadcast_in_dim.51
  288.1 4.4 %all-to-all-start.1 = ((bf16[8,32,2048]{2,1,0:T(8,128)(2,1)}), bf16[8,32,2048]{2,1,0:T(8,128)(2,1)}, u32[]{:S(2)}, u32[]{:S(2)}) async-start(bf16[8,32,2048]{2,1,0:T(8,128)(2,1)} %broadcast_in_dim.51), calls=%async_computation.1 | async-start | bytes 2097152 | tf_op jit(solution)/shard_map/all_to_all | solution.py:40
  292.6 3.5 %copy.37 = bf16[16,1024,64]{1,2,0:T(8,128)(2,1)S(1)} copy(bf16[16,1024,64]{2,1,0:T(8,128)(2,1)} %bitcast.132) | data formatting | bytes 4194304 | tf_op jit(solution)/shard_map/all_gather | solution.py:58
  296.1 4.8 %copy.39 = bf16[16,1024,64]{1,2,0:T(8,128)(2,1)} copy(bf16[16,1024,64]{2,1,0:T(8,128)(2,1)} %bitcast.133) | data formatting | bytes 4194304 | tf_op jit(solution)/shard_map/all_gather | solution.py:58
  300.9 7.4 %all-to-all-done.1 = bf16[8,32,2048]{2,1,0:T(8,128)(2,1)} async-done(((bf16[8,32,2048]{2,1,0:T(8,128)(2,1)}), bf16[8,32,2048]{2,1,0:T(8,128)(2,1)}, u32[]{:S(2)}, u32[]{:S(2)}) %all-to-all-start.1) | async-done | bytes 1048608 | tf_op jit(solution)/shard_map/all_to_all | solution.py:40
  308.3 3.8 %fusion.39 = bf16[256,1024]{1,0:T(8,128)(2,1)S(1)} fusion(bf16[256,2048]{1,0:T(8,128)(2,1)} %bitcast.6, bf16[2048,1024]{1,0:T(8,128)(2,1)} %all-gather.9.cloned.1.call-done), kind=kOutput, calls=%fused_computation.63 | convolution fusion | flops 1074528256 | bytes 5767168 | tf_op jit(solution)/shard_map/dot_general | solution.py:165
  314.6 1.1 copy.40
  316.2 18.4 %all_to_all.16 = bf16[8,32,2048]{2,1,0:T(8,128)(2,1)S(1)} all-to-all(bf16[8,32,2048]{2,1,0:T(8,128)(2,1)S(1)} %convert_element_type.70), channel_id=1, replica_groups=mesh['sp'=16,'tp'=8] {'tp'}, dimensions={0} | all-to-all | bytes 2097152 | tf_op jit(solution)/shard_map/all_to_all | solution.py:34
  (416 shorter events, 69.2 us)
Async XLA Ops:
  6.5 258.4 %copy-start = (bf16[128,2048]{1,0:T(8,128)(2,1)S(1)}, bf16[128,2048]{1,0:T(8,128)(2,1)}, u32[]{:S(2)}) copy-start(bf16[128,2048]{1,0:T(8,128)(2,1)} %param.25) | copy-start | bytes 1572868
  6.5 6.8 %copy-start.4 = (bf16[256,128]{1,0:T(8,128)(2,1)S(1)}, bf16[256,128]{1,0:T(8,128)(2,1)}, u32[]{:S(2)}) copy-start(bf16[256,128]{1,0:T(8,128)(2,1)} %param.16) | copy-start | bytes 196612
  6.5 59.1 %all-gather.7.cloned.1.call-start = ((), (), s32[]{:S(2)}) async-start(), calls=%async_computation.3 | async-start | bytes 5570560 | tf_op jit(solution)/shard_map/all_gather | solution.py:16
  10.0 282.5 %all-gather.11.cloned.1.call-start = ((), (), s32[]{:S(2)}) async-start(), calls=%async_computation.5 | async-start | bytes 4456448 | tf_op jit(solution)/shard_map/all_gather | solution.py:58
  12.0 284.1 %all-gather.13.cloned.1.call-start = ((), (), s32[]{:S(2)}) async-start(), calls=%async_computation.6 | async-start | bytes 4456448 | tf_op jit(solution)/shard_map/all_gather | solution.py:58
  12.8 288.2 %all-gather.9.cloned.1.call-start = ((), (), s32[]{:S(2)}) async-start(), calls=%async_computation.4 | async-start | bytes 4456448 | tf_op jit(solution)/shard_map/all_gather | solution.py:167
  69.3 4.0 %copy-start.6 = (bf16[256,128]{1,0:T(8,128)(2,1)S(1)}, bf16[256,128]{1,0:T(8,128)(2,1)}, u32[]{:S(2)}) copy-start(bf16[256,128]{1,0:T(8,128)(2,1)} %param.19) | copy-start | bytes 196612
  264.9 1.0 copy-start.3
  266.4 20.4 %copy-start.2 = (bf16[32,2048]{1,0:T(8,128)(2,1)S(1)}, bf16[32,2048]{1,0:T(8,128)(2,1)}, u32[]{:S(2)}) copy-start(bf16[32,2048]{1,0:T(8,128)(2,1)} %param.24) | copy-start | bytes 393220
  266.4 20.5 %copy-start.5 = (f32[2048]{0:T(1024)S(1)}, f32[2048]{0:T(1024)}, u32[]{:S(2)}) copy-start(f32[2048]{0:T(1024)} %param.27) | copy-start | bytes 24580
  288.1 20.2 %all-to-all-start.1 = ((bf16[8,32,2048]{2,1,0:T(8,128)(2,1)}), bf16[8,32,2048]{2,1,0:T(8,128)(2,1)}, u32[]{:S(2)}, u32[]{:S(2)}) async-start(bf16[8,32,2048]{2,1,0:T(8,128)(2,1)} %broadcast_in_dim.51), calls=%async_computation.1 | async-start | bytes 2097152 | tf_op jit(solution)/shard_map/all_to_all | solution.py:40
  312.1 1.6 copy-start.1
Sparse Core Ops, SparseCore 0:
  10.2 55.4 all-gather.6
  67.8 51.0 all-gather.10
  121.1 51.0 all-gather.12
  174.2 51.0 all-gather.8
where the time goes:
time: 344 us; the launch traced here: 342 us
  other arithmetic  137 us (40%)
  waiting for transfers between devices  60.9 us (18%)
  local copies, waits for them, and re-layouts  44.4 us (13%)
  matrix products  40.3 us (12%)
  blocking collectives  38.6 us (11%)
  between operations  13.4 us (4%)
  starting transfers between devices  4.56 us (1%)
    another operation x64, other arithmetic  111 us
    all_gather x1, waiting for transfers between devices, turned_gather(): whole = lax.all_gather(both, axis, axis=0, tiled=True)  52.2 us
    all_to_all x2, blocking collectives, summed_on_arrival(): tiles = lax.all_to_all(cut_along(value, dim, count), axis, 0, 0, tiled=True)  38.6 us
    dot_general x32, matrix products, stick_block(): jnp.einsum('qhe,khe->hqk', q_heads, k_heads, preferred_element_type=jnp.f...  28 us
    convert_element_type x32, other arithmetic, stick_block(): weight = weight.astype(jnp.bfloat16)  19.2 us
    dynamic_slice x48, local copies, waits for them, and re-layouts, sweep(): lax.dynamic_slice_in_dim(array, first_row, key_span, 0)  17.7 us
    all_gather x2, local copies, waits for them, and re-layouts, on_gathered_pieces(): tiles = [lax.all_gather(share, axis) for share in pieces]  8.29 us
    all_to_all x1, waiting for transfers between devices, from_everyone(): return lax.all_to_all(copies, axis, split_axis=0, concat_axis=0, tiled=True)  7.39 us
  transfers between devices with their start and end apart: 5, of which 2 were waited for; matrix products, arithmetic and copies ran while one was open for 61% of the time, Pallas kernels for 0%

commit v1 on v0

v1 whole, which is shorter than its diff:
```python
import functools
import heapq

import jax
import jax.numpy as jnp
from jax import lax
from jax.experimental import pallas as pl
from jax.experimental.pallas import tpu as pltpu
from jax.sharding import PartitionSpec as P

MESH = pl.DeviceIdType.MESH
LOG2E = 1.4426950408889634
F32 = jnp.float32
BF16 = jnp.bfloat16

KN, OFF, VN, KB, VB, KV_ROWS = 0, 256, 272, 528, 784, 1040
KV_PARTS = ((KN, 272), (VN, 256), (KB, 256), (VB, 256))


def children(q, dx, dz):
    first, second = (dx, dz) if q < 2 else (dz, dx)
    a, b = ("x", "z") if q < 2 else ("z", "x")
    odd = q % 2
    out = []

    def node(f, s):
        return (f, s) if q < 2 else (s, f)

    if second == 0:
        if first == 0:
            out += [(a, 1, *node(1, 0)), (a, -1, *node(3, 0))]
        elif first == 1 and odd == 0:
            out += [(a, 1, *node(2, 0))]
        elif first == 3 and odd == 1:
            out += [(a, -1, *node(2, 0))]
    if second == 0:
        out += [(b, 1, *node(first, 1)), (b, -1, *node(first, 3))]
    elif second == 1 and odd == 0:
        out += [(b, 1, *node(first, 2))]
    elif second == 3 and odd == 1:
        out += [(b, -1, *node(first, 2))]
    return out


def own_sends():
    firsts, rest = [], []
    for q in range(4):
        a = "x" if q < 2 else "z"
        for child in children(q, 0, 0):
            (firsts if child[0] == a else rest).append((q, *child))
    return firsts + rest


def arrivals():
    free = {}
    queue = []

    def send(now, q, axis, step, dx, dz):
        start = max(now, free.get((axis, step), 0.0))
        free[axis, step] = start + 1.4
        heapq.heappush(queue, (start + 1.4 + 1.7, q, dx, dz))

    for entry in own_sends():
        send(0.0, *entry)
    order = []
    while queue:
        now, q, dx, dz = heapq.heappop(queue)
        order.append((q, dx, dz))
        for child in children(q, dx, dz):
            send(now, q, *child)
    return order


ORDER = arrivals()


def body(
    qn_hbm, kn_hbm, vn_hbm, qb_hbm, kb_hbm, vb_hbm, offn_ref, offb_ref, res_hbm,
    on_hbm, ob_hbm, gain_ref, up_hbm, down_hbm, out_ref,
    kv_buf, up_buf, down_buf, q_buf, res_buf, outw_buf, tri_buf, acc_buf,
    part_buf, pair_buf, sum_buf, mid_in, mid_out, last_out, last_in,
    upd_buf, norm_buf, hidden_buf,
    load_sem, recv_sem, send_sem, pair_sem, mid_sem, last_sem, row_sem, y_send,
):
    s = lax.axis_index("sp")
    t = lax.axis_index("tp")
    x, z = lax.rem(s, 4), lax.div(s, 4)
    c, y = lax.rem(t, 2), lax.div(t, 2)

    def xz(dx, dz):
        return lax.rem(z + dz + 4, 4) * 4 + lax.rem(x + dx + 4, 4)

    def at_tp(dy):
        return lax.rem(y + dy + 4, 4) * 2 + c

    neighbour = {
        ("x", 1): {"sp": xz(1, 0), "tp": t},
        ("x", -1): {"sp": xz(-1, 0), "tp": t},
        ("z", 1): {"sp": xz(0, 1), "tp": t},
        ("z", -1): {"sp": xz(0, -1), "tp": t},
        "pair": {"sp": s, "tp": y * 2 + (1 - c)},
        ("y", 1): {"sp": s, "tp": at_tp(1)},
        ("y", -1): {"sp": s, "tp": at_tp(-1)},
    }

    own = pl.multiple_of(s * 128, 128)
    loads = [
        (kn_hbm, kv_buf.at[s, pl.ds(KN, 256)]),
        (vn_hbm, kv_buf.at[s, pl.ds(VN, 256)]),
        (kb_hbm, kv_buf.at[s, pl.ds(KB, 256)]),
        (vb_hbm, kv_buf.at[s, pl.ds(VB, 256)]),
        (up_hbm, up_buf.at[pl.ds(own, 128)]),
        (down_hbm, down_buf.at[s]),
        (qn_hbm, q_buf.at[0]),
        (qb_hbm, q_buf.at[1]),
        (on_hbm, outw_buf.at[pl.ds(0, 128)]),
        (ob_hbm, outw_buf.at[pl.ds(128, 128)]),
        (res_hbm, res_buf),
    ]
    loads = [pltpu.make_async_copy(a, b, load_sem.at[k]) for k, (a, b) in enumerate(loads)]
    for copy in loads:
        copy.start()

    barrier = pltpu.get_barrier_semaphore()
    for target in neighbour.values():
        pl.semaphore_signal(barrier, inc=1, device_id=target, device_id_type=MESH)

    offsets = [offn_ref[0:1, :], offn_ref[1:2, :], offb_ref[0:1, :]]
    rows = []
    for line in offsets:
        wide = line.astype(F32)
        rows += [wide[:, :128], wide[:, 128:]]
    rows.append(jnp.zeros((10, 128), F32))
    kv_buf[s, OFF : OFF + 16, :] = jnp.concatenate(rows, axis=0).astype(BF16)
    later = lax.broadcasted_iota(jnp.int32, (256, 256), 0)
    earlier = lax.broadcasted_iota(jnp.int32, (256, 256), 1)
    tri_buf[...] = jnp.where(later >= earlier, 1.0, 0.0).astype(BF16)
    pl.semaphore_wait(barrier, 7)

    def piece(g, slot, q):
        if g == 0:
            start, size = KV_PARTS[q]
            return kv_buf.at[slot, pl.ds(start, size)]
        if g == 1:
            return up_buf.at[pl.ds(pl.multiple_of(slot * 128 + q * 32, 32), 32)]
        return down_buf.at[slot, pl.ds(q * 256, 256)]

    def send(g, slot, q, axis, step, dx, dz):
        ref = piece(g, slot, q)
        pltpu.make_async_remote_copy(
            src_ref=ref, dst_ref=ref, send_sem=send_sem.at[g],
            recv_sem=recv_sem.at[g, q, dz * 4 + dx],
            device_id=neighbour[axis, step], device_id_type=MESH,
        ).start()

    def start_gather(g):
        for entry in own_sends():
            send(g, s, *entry)

    def pass_on(g, events):
        for q, dx, dz in events:
            slot = xz(-dx, -dz)
            ref = piece(g, slot, q)
            pltpu.make_async_copy(ref, ref, recv_sem.at[g, q, dz * 4 + dx]).wait()
            for child in children(q, dx, dz):
                send(g, slot, q, *child)

    for copy in loads[:4]:
        copy.wait()
    start_gather(0)
    for copy in loads[4:8]:
        copy.wait()
    lane = lax.broadcasted_iota(jnp.int32, (256, 128), 1)
    acc_buf[...] = jnp.zeros_like(acc_buf)
    pass_on(0, ORDER[:44])
    start_gather(1)
    pass_on(0, ORDER[44:])
    start_gather(2)

    zero = jnp.zeros((), BF16)
    queries = (
        jnp.where(lane < 64, q_buf[0], zero),
        jnp.where(lane >= 64, q_buf[0], zero),
        q_buf[1],
    )
    scales = (LOG2E * 64**-0.5, LOG2E * 64**-0.5, LOG2E * 128**-0.5)

    def attend(slot, kept, diagonal):
        offs = kv_buf[slot, OFF : OFF + 16, :].astype(F32) * LOG2E
        new_kept = []
        for h in range(3):
            k = kv_buf[slot, pl.ds(KN if h < 2 else KB, 256), :]
            v = kv_buf[slot, pl.ds(VN if h < 2 else VB, 256), :]
            if h < 2:
                v = jnp.where((lane < 64) if h == 0 else (lane >= 64), v, zero)
            scores = lax.dot_general(queries[h], k, (((1,), (1,)), ((), ())), preferred_element_type=F32)
            off = jnp.concatenate([offs[2 * h : 2 * h + 1], offs[2 * h + 1 : 2 * h + 2]], axis=1)
            scores = scores * scales[h] + off
            drop = jnp.maximum(scores, 0.0) + jnp.log2(1.0 + jnp.exp2(-jnp.abs(scores)))
            if diagonal:
                drop = jnp.where(earlier < later, drop, 0.0)
            high = drop.astype(BF16)
            low = (drop - high.astype(F32)).astype(BF16)
            gone = jnp.dot(high, tri_buf[...], preferred_element_type=F32) + jnp.dot(
                low, tri_buf[...], preferred_element_type=F32
            )
            weight = jnp.exp2(scores - gone - kept[h])
            if diagonal:
                weight = jnp.where(earlier < later, weight, 0.0)
            mixed = jnp.dot(weight.astype(BF16), v, preferred_element_type=F32)
            acc_buf[0 if h < 2 else 1] += mixed
            new_kept.append(kept[h] + gone[:, 0:1])
        return tuple(new_kept)

    kept = attend(s, (jnp.zeros((256, 1), F32),) * 3, True)
    lax.fori_loop(0, s, lambda k, kept: attend(s - 1 - k, kept, False), kept)

    for copy in loads[8:]:
        copy.wait()

    def project(a, w, columns, width):
        return jnp.dot(a, w, preferred_element_type=F32)

    def row_block(yy, core):
        return pl.ds(pl.multiple_of((yy * 2 + core) * 32, 32), 32)

    def y_at(dy):
        return lax.rem(y + dy + 4, 4)

    def pair_copy(r):
        return pltpu.make_async_remote_copy(
            src_ref=part_buf.at[r, 1 - c], dst_ref=pair_buf.at[r],
            send_sem=y_send.at[r, 0], recv_sem=pair_sem.at[r],
            device_id=neighbour["pair"], device_id_type=MESH,
        )

    def mid_copy(r, k):
        return pltpu.make_async_remote_copy(
            src_ref=mid_out.at[r, k], dst_ref=mid_in.at[r, k],
            send_sem=y_send.at[r, 1 + k], recv_sem=mid_sem.at[r, k],
            device_id=neighbour["y", 1 if k == 0 else -1], device_id_type=MESH,
        )

    def last_copy(r, k):
        return pltpu.make_async_remote_copy(
            src_ref=last_out.at[r, k], dst_ref=last_in.at[r, k],
            send_sem=y_send.at[r, 3 + k], recv_sem=last_sem.at[r, k],
            device_id=neighbour["y", 1 if k == 0 else -1], device_id_type=MESH,
        )

    def store_part(r, value, columns, width):
        blocks = value.reshape(4, 2, 32, width)
        for core in range(2):
            for yy in range(4):
                part_buf[r, core, yy, :, columns] = blocks[yy, core].astype(BF16)

    def pair_step(r):
        pair_copy(r).wait_recv()
        for yy in range(4):
            sum_buf[yy] = part_buf[r, c, yy].astype(F32) + pair_buf[r, yy].astype(F32)
        far = y_at(2)
        mid_out[r, 0] = sum_buf[far, :, 0:1024].astype(BF16)
        mid_out[r, 1] = sum_buf[far, :, 1024:2048].astype(BF16)
        mid_copy(r, 0).start()
        mid_copy(r, 1).start()

    def mid_step(r):
        mid_copy(r, 0).wait_recv()
        last_out[r, 0, :, 0:1024] = (sum_buf[y_at(1), :, 0:1024] + mid_in[r, 0].astype(F32)).astype(BF16)
        last_out[r, 0, :, 1024:2048] = sum_buf[y_at(1), :, 1024:2048].astype(BF16)
        last_copy(r, 0).start()
        mid_copy(r, 1).wait_recv()
        last_out[r, 1, :, 0:1024] = sum_buf[y_at(-1), :, 0:1024].astype(BF16)
        last_out[r, 1, :, 1024:2048] = (sum_buf[y_at(-1), :, 1024:2048] + mid_in[r, 1].astype(F32)).astype(BF16)
        last_copy(r, 1).start()

    def last_step(r):
        last_copy(r, 0).wait_recv()
        last_copy(r, 1).wait_recv()
        return sum_buf[y] + last_in[r, 0].astype(F32) + last_in[r, 1].astype(F32)

    mixed = jnp.concatenate([acc_buf[0], acc_buf[1]], axis=1).astype(BF16)

    @pl.loop(0, 4)
    def _(n):
        columns = pl.ds(pl.multiple_of(n * 512, 512), 512)
        store_part(0, jnp.dot(mixed, outw_buf[:, columns], preferred_element_type=F32), columns, 512)

    pair_copy(0).start()
    pass_on(1, ORDER[:16])
    pair_step(0)
    pass_on(1, ORDER[16:28])
    mid_step(0)
    pass_on(1, ORDER[28:36])
    updated = res_buf[...].astype(F32) + last_step(0)
    upd_buf[...] = updated
    scale = lax.rsqrt(jnp.mean(updated * updated, axis=-1, keepdims=True) + 1e-06)
    norm_buf[t] = (updated * scale * gain_ref[...]).astype(BF16)

    def row_copy(ref, target, k):
        return pltpu.make_async_remote_copy(
            src_ref=ref, dst_ref=ref, send_sem=y_send.at[2, k], recv_sem=row_sem.at[k],
            device_id=neighbour[target], device_id_type=MESH,
        )

    here = norm_buf.at[t]
    up_one = norm_buf.at[y_at(-1) * 2 + c]
    down_one = norm_buf.at[y_at(1) * 2 + c]
    far_top = norm_buf.at[y_at(2) * 2 + c, pl.ds(0, 16)]
    far_low = norm_buf.at[y_at(2) * 2 + c, pl.ds(16, 16)]
    first = [row_copy(here, ("y", 1), 0), row_copy(here, ("y", -1), 1), row_copy(here, "pair", 2)]
    for copy in first:
        copy.start()
    pass_on(1, ORDER[36:46])

    def row_wait(ref, k):
        pltpu.make_async_copy(ref, ref, row_sem.at[k]).wait()

    sent = list(first)

    def forward(ref, target, k):
        copy = row_copy(ref, target, k)
        copy.start()
        sent.append(copy)

    row_wait(up_one, 0)
    forward(norm_buf.at[y_at(-1) * 2 + c, pl.ds(0, 16)], ("y", 1), 3)
    forward(up_one, "pair", 5)
    row_wait(down_one, 1)
    forward(norm_buf.at[y_at(1) * 2 + c, pl.ds(16, 16)], ("y", -1), 4)
    forward(down_one, "pair", 6)
    pass_on(1, ORDER[46:60])
    row_wait(far_top, 3)
    forward(far_top, "pair", 7)
    row_wait(far_low, 4)
    forward(far_low, "pair", 8)
    pass_on(2, ORDER[:16])
    other = 1 - c
    row_wait(norm_buf.at[y * 2 + other], 2)
    row_wait(norm_buf.at[y_at(-1) * 2 + other], 5)
    row_wait(norm_buf.at[y_at(1) * 2 + other], 6)
    row_wait(norm_buf.at[y_at(2) * 2 + other, pl.ds(0, 16)], 7)
    row_wait(norm_buf.at[y_at(2) * 2 + other, pl.ds(16, 16)], 8)

    @pl.loop(0, 4)
    def _(n):
        columns = pl.ds(pl.multiple_of(n * 256, 256), 256)
        rows = norm_buf[...].reshape(256, 2048)
        pre = jnp.maximum(jnp.dot(rows, up_buf[:, columns], preferred_element_type=F32), 0.0)
        hidden_buf[:, columns] = (pre * pre).astype(BF16)

    pass_on(2, ORDER[16:])

    @pl.loop(0, 8)
    def _(n):
        w = jnp.concatenate([down_buf[2 * n], down_buf[2 * n + 1]], axis=1)
        value = jnp.dot(hidden_buf[...], w, preferred_element_type=F32)
        store_part(1, value, pl.ds(pl.multiple_of(n * 256, 256), 256), 256)

    pair_copy(1).start()
    pair_step(1)
    mid_step(1)
    out_ref[...] = (upd_buf[...] + last_step(1)).astype(BF16)

    for r in range(2):
        pair_copy(r).wait_send()
        for k in range(2):
            mid_copy(r, k).wait_send()
            last_copy(r, k).wait_send()
    for copy in sent:
        copy.wait_send()
    for g, ref in enumerate((kv_buf.at[pl.ds(0, 15)], up_buf.at[pl.ds(0, 1920)], down_buf.at[pl.ds(0, 15)])):
        pltpu.make_async_copy(ref, ref, send_sem.at[g]).wait()


def local(qn, kn, vn, qb, kb, vb, offn, offb, res, on, ob, gain, up, down):
    hbm = pl.BlockSpec(memory_space=pl.ANY)
    vmem = pl.BlockSpec(memory_space=pltpu.VMEM)
    dma = pltpu.SemaphoreType.DMA
    return pl.pallas_call(
        body,
        out_shape=jax.ShapeDtypeStruct((32, 2048), BF16),
        in_specs=[hbm, hbm, hbm, hbm, hbm, hbm, vmem, vmem, hbm, hbm, hbm, vmem, hbm, hbm],
        out_specs=vmem,
        scratch_shapes=[
            pltpu.VMEM((16, KV_ROWS, 128), BF16),
            pltpu.VMEM((2048, 1024), BF16),
            pltpu.VMEM((16, 1024, 128), BF16),
            pltpu.VMEM((2, 256, 128), BF16),
            pltpu.VMEM((32, 2048), BF16),
            pltpu.VMEM((256, 2048), BF16),
            pltpu.VMEM((256, 256), BF16),
            pltpu.VMEM((2, 256, 128), F32),
            pltpu.VMEM((2, 2, 4, 32, 2048), BF16),
            pltpu.VMEM((2, 4, 32, 2048), BF16),
            pltpu.VMEM((4, 32, 2048), F32),
            pltpu.VMEM((2, 2, 32, 1024), BF16),
            pltpu.VMEM((2, 2, 32, 1024), BF16),
            pltpu.VMEM((2, 2, 32, 2048), BF16),
            pltpu.VMEM((2, 2, 32, 2048), BF16),
            pltpu.VMEM((32, 2048), F32),
            pltpu.VMEM((8, 32, 2048), BF16),
            pltpu.VMEM((256, 1024), BF16),
            dma((11,)),
            dma((3, 4, 16)),
            dma((3,)),
            dma((2,)),
            dma((2, 2)),
            dma((2, 2)),
            dma((9,)),
            dma((3, 9)),
        ],
        compiler_params=pltpu.CompilerParams(
            collective_id=0, has_side_effects=True, vmem_limit_bytes=60 * 1024 * 1024
        ),
    )(qn, kn, vn, qb, kb, vb, offn, offb, res, on, ob, gain.reshape(1, 2048), up, down)


def solution(mesh):
    return jax.shard_map(
        local,
        mesh=mesh,
        in_specs=(
            P("sp", "tp"), P("sp", "tp"), P("sp", "tp"), P("sp", "tp"), P("sp", "tp"), P("sp", "tp"),
            P("tp", "sp"), P("tp", "sp"), P(("sp", "tp"), None), P("tp", None), P("tp", None), P(),
            P("sp", "tp"), P("tp", "sp"),
        ),
        out_specs=P(("sp", "tp"), None),
        check_vma=False,
    )
```

time: 344 us -> 115 us (0.33)
  the two profiles are of different devices: /device:TPU:102 before, /device:TPU:0 now
where the time goes in v1:
time: 115 us; the launch traced here: 114 us
  Pallas kernels  112 us (97%)
  local copies, waits for them, and re-layouts  1.57 us (1%)
    pallas_call x1, Pallas kernels, local(): pl.pallas_call(body, out_shape=jax.ShapeDtypeStruct((32, 2048), BF16), in...  112 us

profile of v1, /device:TPU:0, one launch (start us, length us, event | category | flops | bytes accessed | tf_op | source)
XLA Modules:
  0.0 113.9 jit_solution(8263422171659721956)
XLA Ops:
  0.0 112.3 %shard_map.136 = bf16[32,2048]{1,0:T(8,128)(2,1)} custom-call(bf16[256,128]{1,0:T(8,128)(2,1)} %qn_hbm.1, bf16[256,128]{1,0:T(8,128)(2,1)} %kn_hbm.1, bf16[256,128]{1,0:T(8,128)(2,1)} %vn_hbm.1, bf16[256,128]{1,0:T(8,128)(2,1)} %qb_hbm.1, bf16[256,128]{1,0:T(8,128)(2,1)} %kb_hbm.1, bf16[256,128]{1,0:T(8,128)(2,1)} %vb_hbm.1, bf16[2,256]{1,0:T(2,128)(2,1)} %offn_ref.1, ...), custom_call_target="tpu_custom_call" | custom-call | tf_op jit(solution)/shard_map/pallas_call | solution.py:380
  112.3 1.6 %copy.16 = bf16[32,2048]{1,0:T(8,128)(2,1)} copy(bf16[32,2048]{1,0:T(8,128)(2,1)} %shard_map.136) | data formatting | bytes 262144

commit v2 on v1

--- a/solution.py
+++ b/solution.py
@@ -74,13 +74,23 @@
 ORDER = arrivals()
 
 
+def after_rows(rows):
+    return 1 + max(i for i, (q, dx, dz) in enumerate(ORDER) if dz in rows)
+
+
+ROW0, ROW1 = after_rows((0,)), after_rows((0, 1))
+N1, N2, N3, N4 = 8, 16, 24, 36
+FIRST = [e for e in ORDER if e[1:] in ((0, 1), (0, 3), (1, 0), (3, 0))]
+REST = [e for e in ORDER if e not in FIRST]
+
+
 def body(
     qn_hbm, kn_hbm, vn_hbm, qb_hbm, kb_hbm, vb_hbm, offn_ref, offb_ref, res_hbm,
     on_hbm, ob_hbm, gain_ref, up_hbm, down_hbm, out_ref,
-    kv_buf, up_buf, down_buf, q_buf, res_buf, outw_buf, tri_buf, acc_buf,
+    kv_buf, up_buf, down_buf, q_buf, head_buf, kept_buf, res_buf, outw_buf, tri_buf, acc_buf,
     part_buf, pair_buf, sum_buf, mid_in, mid_out, last_out, last_in,
     upd_buf, norm_buf, hidden_buf,
-    load_sem, recv_sem, send_sem, pair_sem, mid_sem, last_sem, row_sem, y_send,
+    load_sem, recv_sem, send_sem, pair_sem, mid_sem, last_sem, row_sem, row_send, y_send,
 ):
     s = lax.axis_index("sp")
     t = lax.axis_index("tp")
@@ -171,49 +181,53 @@
     for copy in loads[4:8]:
         copy.wait()
     lane = lax.broadcasted_iota(jnp.int32, (256, 128), 1)
+    zero = jnp.zeros((), BF16)
     acc_buf[...] = jnp.zeros_like(acc_buf)
-    pass_on(0, ORDER[:44])
-    start_gather(1)
-    pass_on(0, ORDER[44:])
-    start_gather(2)
-
-    zero = jnp.zeros((), BF16)
-    queries = (
-        jnp.where(lane < 64, q_buf[0], zero),
-        jnp.where(lane >= 64, q_buf[0], zero),
-        q_buf[1],
-    )
+    kept_buf[...] = jnp.zeros_like(kept_buf)
+    head_buf[0] = jnp.where(lane < 64, q_buf[0], zero)
+    head_buf[1] = jnp.where(lane >= 64, q_buf[0], zero)
+    head_buf[2] = q_buf[1]
     scales = (LOG2E * 64**-0.5, LOG2E * 64**-0.5, LOG2E * 128**-0.5)
 
-    def attend(slot, kept, diagonal):
+    def attend(slot, diagonal=False):
         offs = kv_buf[slot, OFF : OFF + 16, :].astype(F32) * LOG2E
-        new_kept = []
+        scores, gone, out = [], [], [[], []]
         for h in range(3):
             k = kv_buf[slot, pl.ds(KN if h < 2 else KB, 256), :]
+            product = lax.dot_general(head_buf[h], k, (((1,), (1,)), ((), ())), preferred_element_type=F32)
+            off = jnp.concatenate([offs[2 * h : 2 * h + 1], offs[2 * h + 1 : 2 * h + 2]], axis=1)
+            scores.append(product * scales[h] + off)
+        for h in range(3):
+            drop = jnp.maximum(scores[h], lax.log2(1.0 + lax.exp2(jnp.minimum(scores[h], 126.0))))
+            if diagonal:
+                drop = jnp.where(earlier < later, drop, 0.0)
+            gone.append(jnp.dot(drop.astype(BF16), tri_buf[...], preferred_element_type=F32))
+        for h in range(3):
+            kept = kept_buf[h]
+            weight = lax.exp2(scores[h] - gone[h] - jnp.concatenate([kept, kept], axis=1))
+            if diagonal:
+                weight = jnp.where(earlier < later, weight, 0.0)
+            kept_buf[h] = kept + jnp.broadcast_to(gone[h][:, 0:1], (256, 128))
             v = kv_buf[slot, pl.ds(VN if h < 2 else VB, 256), :]
             if h < 2:
                 v = jnp.where((lane < 64) if h == 0 else (lane >= 64), v, zero)
-            scores = lax.dot_general(queries[h], k, (((1,), (1,)), ((), ())), preferred_element_type=F32)
-            off = jnp.concatenate([offs[2 * h : 2 * h + 1], offs[2 * h + 1 : 2 * h + 2]], axis=1)
-            scores = scores * scales[h] + off
-            drop = jnp.maximum(scores, 0.0) + jnp.log2(1.0 + jnp.exp2(-jnp.abs(scores)))
-            if diagonal:
-                drop = jnp.where(earlier < later, drop, 0.0)
-            high = drop.astype(BF16)
-            low = (drop - high.astype(F32)).astype(BF16)
-            gone = jnp.dot(high, tri_buf[...], preferred_element_type=F32) + jnp.dot(
-                low, tri_buf[...], preferred_element_type=F32
-            )
-            weight = jnp.exp2(scores - gone - kept[h])
-            if diagonal:
-                weight = jnp.where(earlier < later, weight, 0.0)
-            mixed = jnp.dot(weight.astype(BF16), v, preferred_element_type=F32)
-            acc_buf[0 if h < 2 else 1] += mixed
-            new_kept.append(kept[h] + gone[:, 0:1])
-        return tuple(new_kept)
-
-    kept = attend(s, (jnp.zeros((256, 1), F32),) * 3, True)
-    lax.fori_loop(0, s, lambda k, kept: attend(s - 1 - k, kept, False), kept)
+            out[h // 2].append((weight.astype(BF16), v))
+        for g in range(2):
+            total = acc_buf[g]
+            for weight, v in out[g]:
+                total = total + jnp.dot(weight, v, preferred_element_type=F32)
+            acc_buf[g] = total
+
+    attend(s, True)
+    pass_on(0, ORDER[:ROW0])
+    pl.loop(0, x)(lambda k: attend(s - 1 - k))
+    pass_on(0, ORDER[ROW0:ROW1])
+    start_gather(1)
+    pl.loop(0, jnp.minimum(z, 1) * 4)(lambda k: attend(z * 4 - 1 - k))
+    pass_on(0, ORDER[ROW1:])
+    start_gather(2)
+    pl.loop(0, jnp.maximum(z - 1, 0) * 4)(lambda k: attend(z * 4 - 5 - k))
+    pass_on(1, FIRST)
 
     for copy in loads[8:]:
         copy.wait()
@@ -227,71 +241,89 @@
     def y_at(dy):
         return lax.rem(y + dy + 4, 4)
 
+    widths = (2048, 512, 512, 512, 512)
+    starts = (0, 2048, 2560, 3072, 3584)
+
+    def cols(r, lo=0, hi=None):
+        hi = widths[r] if hi is None else hi
+        return pl.ds(starts[r] + lo, hi - lo)
+
+    def half_cols(r, k=0):
+        return pl.ds(starts[r] // 2, widths[r] // 2)
+
     def pair_copy(r):
         return pltpu.make_async_remote_copy(
-            src_ref=part_buf.at[r, 1 - c], dst_ref=pair_buf.at[r],
+            src_ref=part_buf.at[1 - c, :, :, cols(r)], dst_ref=pair_buf.at[:, :, cols(r)],
             send_sem=y_send.at[r, 0], recv_sem=pair_sem.at[r],
             device_id=neighbour["pair"], device_id_type=MESH,
         )
 
     def mid_copy(r, k):
         return pltpu.make_async_remote_copy(
-            src_ref=mid_out.at[r, k], dst_ref=mid_in.at[r, k],
+            src_ref=mid_out.at[k, :, half_cols(r)], dst_ref=mid_in.at[k, :, half_cols(r)],
             send_sem=y_send.at[r, 1 + k], recv_sem=mid_sem.at[r, k],
             device_id=neighbour["y", 1 if k == 0 else -1], device_id_type=MESH,
         )
 
     def last_copy(r, k):
         return pltpu.make_async_remote_copy(
-            src_ref=last_out.at[r, k], dst_ref=last_in.at[r, k],
+            src_ref=last_out.at[k, :, cols(r)], dst_ref=last_in.at[k, :, cols(r)],
             send_sem=y_send.at[r, 3 + k], recv_sem=last_sem.at[r, k],
             device_id=neighbour["y", 1 if k == 0 else -1], device_id_type=MESH,
         )
 
-    def store_part(r, value, columns, width):
+    def store_part(value, columns, width):
         blocks = value.reshape(4, 2, 32, width)
         for core in range(2):
             for yy in range(4):
-                part_buf[r, core, yy, :, columns] = blocks[yy, core].astype(BF16)
+                part_buf[core, yy, :, columns] = blocks[yy, core].astype(BF16)
 
     def pair_step(r):
         pair_copy(r).wait_recv()
+        half = widths[r] // 2
         for yy in range(4):
-            sum_buf[yy] = part_buf[r, c, yy].astype(F32) + pair_buf[r, yy].astype(F32)
+            sum_buf[yy, :, cols(r)] = (
+                part_buf[c, yy, :, cols(r)].astype(F32) + pair_buf[yy, :, cols(r)].astype(F32)
+            )
         far = y_at(2)
-        mid_out[r, 0] = sum_buf[far, :, 0:1024].astype(BF16)
-        mid_out[r, 1] = sum_buf[far, :, 1024:2048].astype(BF16)
+        mid_out[0, :, half_cols(r)] = sum_buf[far, :, cols(r, 0, half)].astype(BF16)
+        mid_out[1, :, half_cols(r)] = sum_buf[far, :, cols(r, half)].astype(BF16)
         mid_copy(r, 0).start()
         mid_copy(r, 1).start()
 
     def mid_step(r):
-        mid_copy(r, 0).wait_recv()
-        last_out[r, 0, :, 0:1024] = (sum_buf[y_at(1), :, 0:1024] + mid_in[r, 0].astype(F32)).astype(BF16)
-        last_out[r, 0, :, 1024:2048] = sum_buf[y_at(1), :, 1024:2048].astype(BF16)
-        last_copy(r, 0).start()
-        mid_copy(r, 1).wait_recv()
-        last_out[r, 1, :, 0:1024] = sum_buf[y_at(-1), :, 0:1024].astype(BF16)
-        last_out[r, 1, :, 1024:2048] = (sum_buf[y_at(-1), :, 1024:2048] + mid_in[r, 1].astype(F32)).astype(BF16)
-        last_copy(r, 1).start()
+        half = widths[r] // 2
+        for k, dy in ((0, 1), (1, -1)):
+            to = y_at(dy)
+            mid_copy(r, k).wait_recv()
+            left = sum_buf[to, :, cols(r, 0, half)]
+            right = sum_buf[to, :, cols(r, half)]
+            passing = mid_in[k, :, half_cols(r)].astype(F32)
+            left, right = (left + passing, right) if k == 0 else (left, right + passing)
+            last_out[k, :, cols(r, 0, half)] = left.astype(BF16)
+            last_out[k, :, cols(r, half)] = right.astype(BF16)
+            last_copy(r, k).start()
 
     def last_step(r):
         last_copy(r, 0).wait_recv()
         last_copy(r, 1).wait_recv()
-        return sum_buf[y] + last_in[r, 0].astype(F32) + last_in[r, 1].astype(F32)
+        return (
+            sum_buf[y, :, cols(r)] + last_in[0, :, cols(r)].astype(F32) + last_in[1, :, cols(r)].astype(F32)
+        )
 
     mixed = jnp.concatenate([acc_buf[0], acc_buf[1]], axis=1).astype(BF16)
 
     @pl.loop(0, 4)
     def _(n):
         columns = pl.ds(pl.multiple_of(n * 512, 512), 512)
-        store_part(0, jnp.dot(mixed, outw_buf[:, columns], preferred_element_type=F32), columns, 512)
+        store_part(jnp.dot(mixed, outw_buf[:, columns], preferred_element_type=F32), columns, 512)
 
     pair_copy(0).start()
-    pass_on(1, ORDER[:16])
+    pass_on(2, FIRST[:8])
     pair_step(0)
-    pass_on(1, ORDER[16:28])
+    pass_on(1, REST[:N1])
     mid_step(0)
-    pass_on(1, ORDER[28:36])
+    pass_on(1, REST[N1:N2])
     updated = res_buf[...].astype(F32) + last_step(0)
     upd_buf[...] = updated
     scale = lax.rsqrt(jnp.mean(updated * updated, axis=-1, keepdims=True) + 1e-06)
@@ -299,7 +331,7 @@
 
     def row_copy(ref, target, k):
         return pltpu.make_async_remote_copy(
-            src_ref=ref, dst_ref=ref, send_sem=y_send.at[2, k], recv_sem=row_sem.at[k],
+            src_ref=ref, dst_ref=ref, send_sem=row_send.at[k], recv_sem=row_sem.at[k],
             device_id=neighbour[target], device_id_type=MESH,
         )
 
@@ -311,7 +343,7 @@
     first = [row_copy(here, ("y", 1), 0), row_copy(here, ("y", -1), 1), row_copy(here, "pair", 2)]
     for copy in first:
         copy.start()
-    pass_on(1, ORDER[36:46])
+    pass_on(1, REST[N2:N3])
 
     def row_wait(ref, k):
         pltpu.make_async_copy(ref, ref, row_sem.at[k]).wait()
@@ -329,12 +361,13 @@
     row_wait(down_one, 1)
     forward(norm_buf.at[y_at(1) * 2 + c, pl.ds(16, 16)], ("y", -1), 4)
     forward(down_one, "pair", 6)
-    pass_on(1, ORDER[46:60])
+    pass_on(1, REST[N3:N4])
+    pass_on(2, FIRST[8:])
     row_wait(far_top, 3)
     forward(far_top, "pair", 7)
     row_wait(far_low, 4)
     forward(far_low, "pair", 8)
-    pass_on(2, ORDER[:16])
+    pass_on(1, REST[N4:])
     other = 1 - c
     row_wait(norm_buf.at[y * 2 + other], 2)
     row_wait(norm_buf.at[y_at(-1) * 2 + other], 5)
@@ -349,20 +382,42 @@
         pre = jnp.maximum(jnp.dot(rows, up_buf[:, columns], preferred_element_type=F32), 0.0)
         hidden_buf[:, columns] = (pre * pre).astype(BF16)
 
-    pass_on(2, ORDER[16:])
-
-    @pl.loop(0, 8)
-    def _(n):
-        w = jnp.concatenate([down_buf[2 * n], down_buf[2 * n + 1]], axis=1)
-        value = jnp.dot(hidden_buf[...], w, preferred_element_type=F32)
-        store_part(1, value, pl.ds(pl.multiple_of(n * 256, 256), 256), 256)
-
-    pair_copy(1).start()
-    pair_step(1)
-    mid_step(1)
-    out_ref[...] = (upd_buf[...] + last_step(1)).astype(BF16)
-
-    for r in range(2):
+    def mixer_sums(r, dz):
+        zz = lax.rem(z - dz + 4, 4)
+        for pair in range(2):
+            slot = zz * 4 + pair * 2
+            w = jnp.concatenate([down_buf[slot], down_buf[slot + 1]], axis=1)
+            value = jnp.dot(hidden_buf[...], w, preferred_element_type=F32)
+            store_part(value, pl.ds(starts[r] + pair * 256, 256), 256)
+        pair_copy(r).start()
+
+    def finish(r, dz):
+        columns = pl.ds(pl.multiple_of(lax.rem(z - dz + 4, 4) * 512, 512), 512)
+        out_ref[:, columns] = (upd_buf[:, columns] + last_step(r)).astype(BF16)
+
+    done = 0
+    rounds = ((1, 0), (2, 1), (3, 3), (4, 2))
+    rest_down = REST
+    for i, (r, dz) in enumerate(rounds):
+        need = 1 + max(k for k, e in enumerate(rest_down) if e[2] == dz)
+        if need > done:
+            pass_on(2, rest_down[done:need])
+            done = need
+        mixer_sums(r, dz)
+        if i >= 1:
+            pair_step(r - 1)
+        if i >= 2:
+            mid_step(r - 2)
+        if i >= 3:
+            finish(*rounds[i - 3])
+    pair_step(4)
+    mid_step(3)
+    finish(*rounds[1])
+    mid_step(4)
+    finish(*rounds[2])
+    finish(*rounds[3])
+
+    for r in range(5):
         pair_copy(r).wait_send()
         for k in range(2):
             mid_copy(r, k).wait_send()
@@ -387,28 +442,31 @@
             pltpu.VMEM((2048, 1024), BF16),
             pltpu.VMEM((16, 1024, 128), BF16),
             pltpu.VMEM((2, 256, 128), BF16),
+            pltpu.VMEM((3, 256, 128), BF16),
+            pltpu.VMEM((3, 256, 128), F32),
             pltpu.VMEM((32, 2048), BF16),
             pltpu.VMEM((256, 2048), BF16),
             pltpu.VMEM((256, 256), BF16),
             pltpu.VMEM((2, 256, 128), F32),
-            pltpu.VMEM((2, 2, 4, 32, 2048), BF16),
-            pltpu.VMEM((2, 4, 32, 2048), BF16),
-            pltpu.VMEM((4, 32, 2048), F32),
-            pltpu.VMEM((2, 2, 32, 1024), BF16),
-            pltpu.VMEM((2, 2, 32, 1024), BF16),
-            pltpu.VMEM((2, 2, 32, 2048), BF16),
-            pltpu.VMEM((2, 2, 32, 2048), BF16),
+            pltpu.VMEM((2, 4, 32, 4096), BF16),
+            pltpu.VMEM((4, 32, 4096), BF16),
+            pltpu.VMEM((4, 32, 4096), F32),
+            pltpu.VMEM((2, 32, 2048), BF16),
+            pltpu.VMEM((2, 32, 2048), BF16),
+            pltpu.VMEM((2, 32, 4096), BF16),
+            pltpu.VMEM((2, 32, 4096), BF16),
             pltpu.VMEM((32, 2048), F32),
             pltpu.VMEM((8, 32, 2048), BF16),
             pltpu.VMEM((256, 1024), BF16),
             dma((11,)),
             dma((3, 4, 16)),
             dma((3,)),
-            dma((2,)),
-            dma((2, 2)),
-            dma((2, 2)),
+            dma((5,)),
+            dma((5, 2)),
+            dma((5, 2)),
             dma((9,)),
-            dma((3, 9)),
+            dma((9,)),
+            dma((5, 5)),
         ],
         compiler_params=pltpu.CompilerParams(
             collective_id=0, has_side_effects=True, vmem_limit_bytes=60 * 1024 * 1024

time: 115 us -> 94.6 us (0.82)
  Pallas kernels: 112 us -> 92.9 us
    pallas_call x1, Pallas kernels: 112 us -> 92.9 us  [local(): pl.pallas_call(body, out_shape=jax.ShapeDtypeStruct((32, 2048), BF16), in...]
where the time goes in v2:
time: 94.6 us; the launch traced here: 94.4 us
  Pallas kernels  92.9 us (98%)
  local copies, waits for them, and re-layouts  1.57 us (2%)
    pallas_call x1, Pallas kernels, local(): pl.pallas_call(body, out_shape=jax.ShapeDtypeStruct((32, 2048), BF16), in...  92.9 us

profile of v2, /device:TPU:0, one launch (start us, length us, event | category | flops | bytes accessed | tf_op | source)
XLA Modules:
  0.0 94.4 jit_solution(8451276416566034781)
XLA Ops:
  0.0 92.9 %shard_map.136 = bf16[32,2048]{1,0:T(8,128)(2,1)} custom-call(bf16[256,128]{1,0:T(8,128)(2,1)} %qn_hbm.1, bf16[256,128]{1,0:T(8,128)(2,1)} %kn_hbm.1, bf16[256,128]{1,0:T(8,128)(2,1)} %vn_hbm.1, bf16[256,128]{1,0:T(8,128)(2,1)} %qb_hbm.1, bf16[256,128]{1,0:T(8,128)(2,1)} %kb_hbm.1, bf16[256,128]{1,0:T(8,128)(2,1)} %vb_hbm.1, bf16[2,256]{1,0:T(2,128)(2,1)} %offn_ref.1, ...), custom_call_target="tpu_custom_call" | custom-call | tf_op jit(solution)/shard_map/pallas_call | solution.py:435
  92.9 1.6 %copy.16 = bf16[32,2048]{1,0:T(8,128)(2,1)} copy(bf16[32,2048]{1,0:T(8,128)(2,1)} %shard_map.136) | data formatting | bytes 262144

commit v3 on v2

v3 whole, which is shorter than its diff:
```python
import functools

import jax
import jax.numpy as jnp
from jax import lax
from jax.experimental import pallas as pl
from jax.experimental.pallas import tpu as pltpu
from jax.sharding import PartitionSpec as P

MESH = pl.DeviceIdType.MESH
LOG2E = 1.4426950408889634
F32 = jnp.float32
BF16 = jnp.bfloat16

OFF, VAL, KV_ROWS = 256, 272, 528


def children(q, dx, dz):
    first, second = (dx, dz) if q < 2 else (dz, dx)
    a, b = ("x", "z") if q < 2 else ("z", "x")
    odd = q % 2
    out = []

    def node(f, s):
        return (f, s) if q < 2 else (s, f)

    if second == 0:
        if first == 0:
            out += [(a, 1, *node(1, 0)), (a, -1, *node(3, 0))]
        elif first == 1 and odd == 0:
            out += [(a, 1, *node(2, 0))]
        elif first == 3 and odd == 1:
            out += [(a, -1, *node(2, 0))]
    if second == 0:
        out += [(b, 1, *node(first, 1)), (b, -1, *node(first, 3))]
    elif second == 1 and odd == 0:
        out += [(b, 1, *node(first, 2))]
    elif second == 3 and odd == 1:
        out += [(b, -1, *node(first, 2))]
    return out


WIRE, DELAY = 6.0, 2.2
POINTS = (
    ("sides", 2.8, 10.0),
    ("keys1", 12.5, 19.0),
    ("keys2", 17.5, 23.0),
    ("att1", 22.0, 25.5),
    ("att2", 24.5, 26.5),
    ("mix1", 28.3, 33.0),
    ("mix2", 30.0, 36.0),
    ("mix3", 35.0, 41.0),
    ("rows0", 38.5, 43.0),
    ("rows1", 42.0, 46.0),
    ("rows2", 43.5, 50.0),
)
SIZES = ((16, 16, 48, 48), (240, 240, 272, 272))
STARTS = ((0, 16, 32, 80), (0, 240, 480, 752))


def plan():
    free = {(axis, step): 0.0 for axis in "xz" for step in (1, -1)}
    landing, backlog, steps = {}, [], {}
    left = {(g, dz): 12 if dz == 0 else 16 for g in range(2) for dz in range(4)}

    def offer(g, q, child):
        first = (child[0] == "x") == (q < 2)
        backlog.append((g, 0 if first else 1, len(backlog), q, child))

    def issue(now, out, until, axes=("x", "z")):
        for entry in sorted(backlog):
            g, _, _, q, child = entry
            axis, step, dx, dz = child
            if axis in axes and free[axis, step] <= until:
                start = max(now, free[axis, step])
                free[axis, step] = start + WIRE * SIZES[g][q] / sum(SIZES[g])
                landing[g, q, dx, dz] = free[axis, step] + DELAY
                out.append(("send", g, q, child))
                backlog.remove(entry)

    def take(out, event):
        g, q, dx, dz = event
        del landing[event]
        left[g, dz] -= 1
        out.append(("wait", g, q, (dx, dz)))
        for child in children(q, dx, dz):
            offer(g, q, child)

    for g in range(2):
        for q in range(4):
            for child in children(q, 0, 0):
                offer(g, q, child)
    for point, now, until in POINTS:
        out = []
        axes = ("x",) if point in ("sides", "keys1") else ("x", "z")
        for when, event in sorted((when, event) for event, when in landing.items()):
            if when <= now - 0.3:
                take(out, event)
        issue(now, out, until, axes)
        steps[point] = out
    order, out = [], []
    while landing or backlog:
        when, event = min((when, event) for event, when in landing.items())
        now = max(now, when)
        take(out, event)
        issue(now, out, now + 6.0)
        if not any(left[0, dz] for dz in range(4)) and "up" not in steps:
            steps["up"] = out
            out = []
        for dz in range(4):
            if "up" in steps and not left[1, dz] and dz not in order:
                order.append(dz)
                steps["row", dz] = out
                out = []
    return steps, order, now


PLAN, ROW_ORDER, PLAN_END = plan()


def body(
    qn_hbm, kn_hbm, vn_hbm, qb_hbm, kb_hbm, vb_hbm, offn_ref, offb_ref, res_hbm,
    on_hbm, ob_hbm, gain_ref, up_hbm, down_hbm, out_ref,
    stage, kv_buf, up_buf, down_buf, outw, q_own, q_all, head_buf, kept_buf, acc_buf, tri_buf,
    mix_out, mix_all, res_buf, att_buf, ex_out, ex_in, part_buf, pair_buf, sum_buf, mid_in, mid_out, last_out, last_in,
    upd_buf, norm_buf, hidden_buf,
    load_sem, recv_sem, send_sem, x_sem, x_send, z_sem, far_sem, kv_send, kvp_sem, kvf_sem,
    q_sem, q_send, m_sem, m_send, ow_sem, ow_send, owp_sem, owp_send, ex_sem, ex_send,
    pair_sem, mid_sem, last_sem, row_sem, row_send, y_send,
):
    s = lax.axis_index("sp")
    t = lax.axis_index("tp")
    x, z = lax.rem(s, 4), lax.div(s, 4)
    c, y = lax.rem(t, 2), lax.div(t, 2)
    part = z * 2 + c
    primary = lax.rem(x, 2) == c
    y_odd = lax.rem(y, 2)
    y_mate = y + 1 - 2 * y_odd
    same_pair = lax.div(z, 2) == lax.div(y, 2)
    mix_y = jnp.where(same_pair, z, 3 - z)
    mix_block = jnp.where(same_pair, jnp.int32(0), jnp.int32(1))
    holds_own = mix_y == y

    def xz(dx, dz):
        return lax.rem(z + dz % 4, 4) * 4 + lax.rem(x + dx % 4, 4)

    def y_at(dy):
        return lax.rem(y + dy + 4, 4)

    def z_at(dz):
        return lax.rem(z + dz + 4, 4)

    neighbour = {
        ("x", 1): {"sp": xz(1, 0), "tp": t},
        ("x", -1): {"sp": xz(-1, 0), "tp": t},
        ("z", 1): {"sp": xz(0, 1), "tp": t},
        ("z", -1): {"sp": xz(0, -1), "tp": t},
        "pair": {"sp": s, "tp": y * 2 + (1 - c)},
        ("y", 1): {"sp": s, "tp": y_at(1) * 2 + c},
        ("y", -1): {"sp": s, "tp": y_at(-1) * 2 + c},
    }

    def remote(src, dst, send, recv, target):
        return pltpu.make_async_remote_copy(
            src_ref=src, dst_ref=dst, send_sem=send, recv_sem=recv, device_id=target, device_id_type=MESH
        )

    def arrived(ref, sem):
        pltpu.make_async_copy(ref, ref, sem).wait()

    own = pl.multiple_of(s * 128, 128)
    loads = [
        (kn_hbm, stage.at[0, pl.ds(0, 256)]),
        (vn_hbm, stage.at[0, pl.ds(VAL, 256)]),
        (kb_hbm, stage.at[1, pl.ds(0, 256)]),
        (vb_hbm, stage.at[1, pl.ds(VAL, 256)]),
        (qn_hbm, q_own.at[0]),
        (qb_hbm, q_own.at[1]),
        (on_hbm, outw.at[y_odd * 4 + c]),
        (ob_hbm, outw.at[y_odd * 4 + 2 + c]),
        (up_hbm, up_buf.at[pl.ds(own, 128)]),
        (down_hbm, down_buf.at[s]),
        (res_hbm, res_buf),
    ]
    loads = [pltpu.make_async_copy(a, b, load_sem.at[k]) for k, (a, b) in enumerate(loads)]
    for copy in loads:
        copy.start()

    mine = [
        [
            pltpu.make_async_copy(k_hbm, kv_buf.at[s, pl.ds(0, 256)], load_sem.at[11]),
            pltpu.make_async_copy(v_hbm, kv_buf.at[s, pl.ds(VAL, 256)], load_sem.at[12]),
            pltpu.make_async_copy(q_hbm.at[pl.ds(pl.multiple_of(part * 32, 32), 32)], q_all.at[s], load_sem.at[13]),
        ]
        for k_hbm, v_hbm, q_hbm in ((kn_hbm, vn_hbm, qn_hbm), (kb_hbm, vb_hbm, qb_hbm))
    ]
    for unit in range(2):

        @pl.when(x == c + 2 * unit)
        def _():
            for copy in mine[unit]:
                copy.start()

    def greet(target, unless=None):
        def signal():
            pl.semaphore_signal(barrier, inc=1, device_id=target, device_id_type=MESH)

        if unless is None:
            signal()
        else:
            pl.when(jnp.logical_not(unless))(signal)

    barrier = pltpu.get_barrier_semaphore()
    for target in neighbour.values():
        greet(target)
    for dz in range(4):
        for dx in range(4):
            here = (dx, dz) == (0, 0)
            greet({"sp": xz(dx, dz), "tp": y * 2 + lax.rem(x, 2)}, primary if here else None)
    for block, rows_z in enumerate((y, 3 - y)):
        for plane in (y, y_mate):
            for dx in range(4):
                here = dx == 0 and plane is y
                greet(
                    {"sp": rows_z * 4 + lax.rem(x + dx, 4), "tp": plane * 2 + c},
                    rows_z == z if here else None,
                )

    offn = offn_ref[...].astype(F32)
    offb = offb_ref[...].astype(F32)
    blank = jnp.zeros((14, 128), F32)
    narrow_rows = [offn[0:1, :128], offn[0:1, 128:], offn[1:2, :128], offn[1:2, 128:], blank[:12]]
    broad_rows = [offb[0:1, :128], offb[0:1, 128:], blank]
    for unit, rows in enumerate((narrow_rows, broad_rows)):
        value = jnp.concatenate(rows, axis=0).astype(BF16)
        stage[unit, OFF : OFF + 16, :] = value

        @pl.when(x == c + 2 * unit)
        def _():
            kv_buf[s, OFF : OFF + 16, :] = value

    later = lax.broadcasted_iota(jnp.int32, (256, 256), 0)
    earlier = lax.broadcasted_iota(jnp.int32, (256, 256), 1)
    tri_buf[...] = jnp.where(later >= earlier, 1.0, 0.0).astype(BF16)
    one, none = jnp.int32(1), jnp.int32(0)
    pl.semaphore_wait(barrier, 39 - jnp.where(primary, one, none) - jnp.where(holds_own, one, none))

    def piece(g, slot, q):
        if g == 0:
            return up_buf.at[pl.ds(pl.multiple_of(slot * 128 + STARTS[0][q], 16), SIZES[0][q])]
        return down_buf.at[slot, pl.ds(STARTS[1][q], SIZES[1][q])]

    def send(g, slot, q, axis, step, dx, dz):
        ref = piece(g, slot, q)
        remote(ref, ref, send_sem.at[g], recv_sem.at[g, q, dz * 4 + dx], neighbour[axis, step]).start()

    def run(point):
        for kind, g, q, what in PLAN[point]:
            if kind == "send":
                axis, step, dx, dz = what
                here = (dx - step, dz) if axis == "x" else (dx, dz - step)
                send(g, xz(-here[0], -here[1]), q, axis, step, dx, dz)
            else:
                dx, dz = what
                arrived(piece(g, xz(-dx, -dz), q), recv_sem.at[g, q, dz * 4 + dx])

    for copy in loads[:4]:
        copy.wait()

    def x_copy(unit):
        col = c + 2 * unit
        return remote(
            stage.at[unit], kv_buf.at[s], x_send.at[unit], x_sem.at[lax.rem(x - col + 4, 4)],
            {"sp": z * 4 + col, "tp": t},
        )

    for unit in range(2):

        @pl.when(x != c + 2 * unit)
        def _():
            x_copy(unit).start()

    def kv_slot(d, dz):
        return xz(d, -dz)

    def to_column(d):
        ref = kv_buf.at[kv_slot(d, 0)]
        remote(ref, ref, kv_send.at[0], z_sem.at[d, 0], neighbour["z", 1]).start()
        remote(ref, ref, kv_send.at[0], z_sem.at[d, 1], neighbour["z", -1]).start()
        remote(ref, ref, kv_send.at[1], kvp_sem.at[d, 0], neighbour["pair"]).start()

    def from_row(d):
        for k, dz in ((0, 1), (1, 3)):
            slot = kv_slot(d, dz)
            ref = kv_buf.at[slot]
            arrived(ref, z_sem.at[d, k])
            half = kv_buf.at[slot, pl.ds(0, VAL) if k == 0 else pl.ds(VAL, 256)]
            remote(half, half, kv_send.at[0], far_sem.at[d, k], neighbour["z", 1 if k == 0 else -1]).start()
            remote(ref, ref, kv_send.at[1], kvp_sem.at[d, dz], neighbour["pair"]).start()

    def far_half(d, k):
        return kv_buf.at[kv_slot(d, 2), pl.ds(0, VAL) if k == 0 else pl.ds(VAL, 256)]

    def from_far(d):
        for k in range(2):
            half = far_half(d, k)
            arrived(half, far_sem.at[d, k])
            remote(half, half, kv_send.at[1], kvf_sem.at[d, k], neighbour["pair"]).start()

    @pl.when(primary)
    def _():
        for unit in range(2):

            @pl.when(x == c + 2 * unit)
            def _():
                for copy in mine[unit]:
                    copy.wait()

        to_column(0)

    for copy in loads[4:8]:
        copy.wait()

    def q_copy(unit, dz, dc):
        core = c if dc == 0 else 1 - c
        rows = pl.ds(pl.multiple_of((z_at(dz) * 2 + core) * 32, 32), 32)
        return remote(
            q_own.at[unit, rows], q_all.at[s], q_send.at[unit, dz, dc], q_sem.at[s],
            {"sp": z_at(dz) * 4 + c + 2 * unit, "tp": y * 2 + core},
        )

    def each_query(act):
        for unit in range(2):
            for dz in range(4):
                for dc in range(2):
                    if (dz, dc) == (0, 0):
                        pl.when(x != c + 2 * unit)(lambda: act(q_copy(unit, dz, dc)))
                    else:
                        act(q_copy(unit, dz, dc))

    each_query(lambda copy: copy.start())

    def ow(k, foreign, core):
        plane = 1 - y_odd if foreign else y_odd
        return outw.at[plane * 4 + core + 2 * k]

    mate = {"sp": s, "tp": y_mate * 2 + c}

    def ow_copy(k):
        return remote(ow(k, 0, c), ow(k, 0, c), ow_send.at[k], ow_sem.at[k], mate)

    def ow_pair(k, foreign):
        ref = ow(k, foreign, c)
        return remote(ref, ref, owp_send.at[k, foreign], owp_sem.at[k, foreign], neighbour["pair"])

    ow_sent = [ow_copy(0), ow_copy(1), ow_pair(0, 0), ow_pair(1, 0)]
    for copy in ow_sent:
        copy.start()

    def ow_pass(k):
        arrived(ow(k, 1, c), ow_sem.at[k])
        copy = ow_pair(k, 1)
        copy.start()
        ow_sent.append(copy)

    loads[8].wait()
    loads[9].wait()
    for unit in range(2):
        pl.when(x != c + 2 * unit)(lambda: x_copy(unit).wait_send())
    run("sides")

    @pl.when(primary)
    def _():
        for d in (1, 3):
            arrived(kv_buf.at[kv_slot(d, 0)], x_sem.at[d])
            to_column(d)
        from_row(0)
        arrived(kv_buf.at[kv_slot(2, 0)], x_sem.at[2])
        to_column(2)
        from_row(1)
        from_row(3)

    run("keys1")

    @pl.when(primary)
    def _():
        from_row(2)
        for d in (0, 1, 3, 2):
            from_far(d)

    @pl.when(jnp.logical_not(primary))
    def _():
        for d in (0, 1, 3, 2):
            for dz in (0, 1, 3):
                arrived(kv_buf.at[kv_slot(d, dz)], kvp_sem.at[d, dz])
            for k in range(2):
                arrived(far_half(d, k), kvf_sem.at[d, k])

    for slot in range(16):
        pl.when(jnp.logical_not(jnp.logical_and(primary, s == slot)))(
            lambda: arrived(q_all.at[slot], q_sem.at[slot])
        )
    ow_pass(0)
    run("keys2")

    lane = lax.broadcasted_iota(jnp.int32, (512, 128), 1)
    zero = jnp.zeros((), BF16)
    acc_buf[...] = jnp.zeros_like(acc_buf)
    kept_buf[...] = jnp.zeros_like(kept_buf)
    queries = q_all[...].reshape(512, 128)
    ahead = (later // 32) * 256 + lax.rem(later, 32) - earlier + part * 32

    def attend(slot, heads, chunks, scale):
        offs = kv_buf[slot, OFF:VAL, :].astype(F32) * LOG2E
        k = kv_buf[slot, pl.ds(0, 256), :]
        v = kv_buf[slot, pl.ds(VAL, 256), :]
        items = [(chunk, masked, h) for chunk, masked in chunks for h in range(heads)]
        scores, gone, weights = [], [], []
        for chunk, masked, h in items:
            product = lax.dot_general(
                head_buf[h, chunk * 256 : chunk * 256 + 256], k, (((1,), (1,)), ((), ())),
                preferred_element_type=F32,
            )
            off = jnp.concatenate([offs[2 * h : 2 * h + 1], offs[2 * h + 1 : 2 * h + 2]], axis=1)
            scores.append(product * scale + off)
        for (chunk, masked, h), score in zip(items, scores):
            drop = jnp.maximum(score, lax.log2(1.0 + lax.exp2(jnp.minimum(score, 126.0))))
            if masked:
                drop = jnp.where(ahead > slot * 256 - chunk * 2048, drop, 0.0)
            gone.append(jnp.dot(drop.astype(BF16), tri_buf[...], preferred_element_type=F32))
        for (chunk, masked, h), score, lost in zip(items, scores, gone):
            rows = slice(chunk * 256, chunk * 256 + 256)
            kept = kept_buf[h, rows]
            weight = lax.exp2(score - lost - jnp.concatenate([kept, kept], axis=1))
            if masked:
                weight = jnp.where(ahead > slot * 256 - chunk * 2048, weight, 0.0)
            kept_buf[h, rows] = kept + jnp.broadcast_to(lost[:, 0:1], (256, 128))
            weights.append(weight.astype(BF16))
        for chunk, _ in chunks:
            rows = slice(chunk * 256, chunk * 256 + 256)
            total = acc_buf[rows]
            for (other, _, h), weight in zip(items, weights):
                if other == chunk:
                    values = v
                    if heads == 2:
                        values = jnp.where((lane[:256] < 64) if h == 0 else (lane[:256] >= 64), v, zero)
                    total = total + jnp.dot(weight, values, preferred_element_type=F32)
            acc_buf[rows] = total

    def attention(heads, scale):
        if heads == 2:
            head_buf[0] = jnp.where(lane < 64, queries, zero)
            head_buf[1] = jnp.where(lane >= 64, queries, zero)
        else:
            head_buf[0] = queries

    def each_group(act):
        pl.when(x < 2)(lambda: act(2, LOG2E * 64**-0.5))
        pl.when(x >= 2)(lambda: act(1, LOG2E * 128**-0.5))

    def late_keys(heads, scale):
        if heads == 2:
            head_buf[0] = jnp.where(lane < 64, queries, zero)
            head_buf[1] = jnp.where(lane >= 64, queries, zero)
        else:
            head_buf[0] = queries
        pl.loop(0, 8)(lambda k: attend(15 - k, heads, ((1, True),), scale))

    def early_keys(first, heads, scale):
        pl.loop(0, 4)(lambda k: attend(first - k, heads, ((0, True), (1, False)), scale))

    each_group(late_keys)
    run("att1")
    each_group(functools.partial(early_keys, 7))
    run("att2")
    each_group(functools.partial(early_keys, 3))

    mix_out[...] = acc_buf[...].reshape(16, 32, 128).astype(BF16)

    def m_copy(dx, dz):
        return remote(
            mix_out.at[xz(dx, dz)], mix_all.at[mix_block, y_odd * 4 + x], m_send.at[dz, dx],
            m_sem.at[mix_block, y_odd * 4 + x], {"sp": xz(dx, dz), "tp": mix_y * 2 + c},
        )

    def each_mixed(act):
        for dz in range(4):
            for dx in range(4):
                if (dx, dz) == (0, 0):
                    pl.when(jnp.logical_not(holds_own))(lambda: act(m_copy(dx, dz)))
                else:
                    act(m_copy(dx, dz))

    each_mixed(lambda copy: copy.start())

    @pl.when(holds_own)
    def _():
        mix_all[mix_block, y_odd * 4 + x] = mix_out[s]

    run("mix1")
    ow_pass(1)
    run("mix2")
    for block in range(2):
        for unit in range(8):
            from_me = jnp.logical_and(holds_own, jnp.logical_and(mix_block == block, y_odd * 4 + x == unit))
            pl.when(jnp.logical_not(from_me))(
                lambda: arrived(mix_all.at[block, unit], m_sem.at[block, unit])
            )
    for k in range(2):
        for foreign in range(2):
            arrived(ow(k, foreign, 1 - c), owp_sem.at[k, foreign])
    loads[10].wait()

    mixed = jnp.concatenate([mix_all[:, unit].reshape(64, 128) for unit in range(8)], axis=1)

    def ex_copy(n):
        columns = pl.ds(n * 512, 512)
        return remote(
            ex_out.at[:, columns], ex_in.at[:, columns], ex_send.at[n], ex_sem.at[n],
            {"sp": s, "tp": (3 - y) * 2 + c},
        )

    for n in range(4):
        columns = slice(n * 512, n * 512 + 512)
        sums = jnp.dot(mixed, outw[:, :, columns].reshape(1024, 512), preferred_element_type=F32)
        att_buf[:, columns] = sums[:32]
        ex_out[:, columns] = sums[32:].astype(BF16)
        ex_copy(n).start()
    run("mix3")
    for n in range(4):
        ex_copy(n).wait_recv()
    updated = res_buf[...].astype(F32) + (att_buf[...] + ex_in[...].astype(F32))
    upd_buf[...] = updated
    scale = lax.rsqrt(jnp.mean(updated * updated, axis=-1, keepdims=True) + 1e-06)
    norm_buf[t] = (updated * scale * gain_ref[...]).astype(BF16)

    def row_copy(ref, target, k):
        return remote(ref, ref, row_send.at[k], row_sem.at[k], neighbour[target])

    def half_rows(dy, k, core=None):
        slot = y_at(dy) * 2 + (c if core is None else core)
        return norm_buf.at[slot, pl.ds(16 * k, 16)]

    sent = []

    def row_send_to(ref, target, k):
        copy = row_copy(ref, target, k)
        copy.start()
        sent.append(copy)

    row_send_to(half_rows(0, 0), ("y", 1), 0)
    row_send_to(half_rows(0, 1), ("y", -1), 1)
    row_send_to(half_rows(0, 1), ("y", 1), 2)
    row_send_to(half_rows(0, 0), ("y", -1), 3)
    row_send_to(norm_buf.at[t], "pair", 6)
    run("rows0")
    arrived(half_rows(-1, 0), row_sem.at[0])
    row_send_to(half_rows(-1, 0), ("y", 1), 4)
    arrived(half_rows(1, 1), row_sem.at[1])
    row_send_to(half_rows(1, 1), ("y", -1), 5)
    row_send_to(half_rows(-1, 0), "pair", 7)
    row_send_to(half_rows(1, 1), "pair", 8)
    run("rows1")
    arrived(half_rows(-1, 1), row_sem.at[2])
    row_send_to(half_rows(-1, 1), "pair", 9)
    arrived(half_rows(1, 0), row_sem.at[3])
    row_send_to(half_rows(1, 0), "pair", 10)
    run("rows2")
    arrived(half_rows(2, 0), row_sem.at[4])
    row_send_to(half_rows(2, 0), "pair", 11)
    arrived(half_rows(2, 1), row_sem.at[5])
    row_send_to(half_rows(2, 1), "pair", 12)
    other = 1 - c
    arrived(norm_buf.at[y * 2 + other], row_sem.at[6])
    for k, (dy, half) in enumerate(((-1, 0), (1, 1), (-1, 1), (1, 0), (2, 0), (2, 1))):
        arrived(half_rows(dy, half, other), row_sem.at[7 + k])

    run("up")
    @pl.loop(0, 4)
    def _(n):
        columns = pl.ds(pl.multiple_of(n * 256, 256), 256)
        rows = norm_buf[...].reshape(256, 2048)
        pre = jnp.maximum(jnp.dot(rows, up_buf[:, columns], preferred_element_type=F32), 0.0)
        hidden_buf[:, columns] = (pre * pre).astype(BF16)

    widths = (512, 512, 512, 512)
    starts = (0, 512, 1024, 1536)

    def cols(r, lo=0, hi=None):
        hi = widths[r] if hi is None else hi
        return pl.ds(starts[r] + lo, hi - lo)

    def half_cols(r, k=0):
        return pl.ds(starts[r] // 2, widths[r] // 2)

    def pair_copy(r):
        return pltpu.make_async_remote_copy(
            src_ref=part_buf.at[1 - c, :, :, cols(r)], dst_ref=pair_buf.at[:, :, cols(r)],
            send_sem=y_send.at[r, 0], recv_sem=pair_sem.at[r],
            device_id=neighbour["pair"], device_id_type=MESH,
        )

    def mid_copy(r, k):
        return pltpu.make_async_remote_copy(
            src_ref=mid_out.at[k, :, half_cols(r)], dst_ref=mid_in.at[k, :, half_cols(r)],
            send_sem=y_send.at[r, 1 + k], recv_sem=mid_sem.at[r, k],
            device_id=neighbour["y", 1 if k == 0 else -1], device_id_type=MESH,
        )

    def last_copy(r, k):
        return pltpu.make_async_remote_copy(
            src_ref=last_out.at[k, :, cols(r)], dst_ref=last_in.at[k, :, cols(r)],
            send_sem=y_send.at[r, 3 + k], recv_sem=last_sem.at[r, k],
            device_id=neighbour["y", 1 if k == 0 else -1], device_id_type=MESH,
        )

    def store_part(value, columns, width):
        blocks = value.reshape(4, 2, 32, width)
        for core in range(2):
            for yy in range(4):
                part_buf[core, yy, :, columns] = blocks[yy, core].astype(BF16)

    def pair_step(r):
        pair_copy(r).wait_recv()
        half = widths[r] // 2
        for yy in range(4):
            sum_buf[yy, :, cols(r)] = (
                part_buf[c, yy, :, cols(r)].astype(F32) + pair_buf[yy, :, cols(r)].astype(F32)
            )
        far = y_at(2)
        mid_out[0, :, half_cols(r)] = sum_buf[far, :, cols(r, 0, half)].astype(BF16)
        mid_out[1, :, half_cols(r)] = sum_buf[far, :, cols(r, half)].astype(BF16)
        mid_copy(r, 0).start()
        mid_copy(r, 1).start()

    def mid_step(r):
        half = widths[r] // 2
        for k, dy in ((0, 1), (1, -1)):
            to = y_at(dy)
            mid_copy(r, k).wait_recv()
            left = sum_buf[to, :, cols(r, 0, half)]
            right = sum_buf[to, :, cols(r, half)]
            passing = mid_in[k, :, half_cols(r)].astype(F32)
            left, right = (left + passing, right) if k == 0 else (left, right + passing)
            last_out[k, :, cols(r, 0, half)] = left.astype(BF16)
            last_out[k, :, cols(r, half)] = right.astype(BF16)
            last_copy(r, k).start()

    def last_step(r):
        last_copy(r, 0).wait_recv()
        last_copy(r, 1).wait_recv()
        return (
            sum_buf[y, :, cols(r)] + last_in[0, :, cols(r)].astype(F32) + last_in[1, :, cols(r)].astype(F32)
        )

    def mixer_sums(r, dz):
        zz = lax.rem(z - dz + 4, 4)
        for pair in range(2):
            slot = zz * 4 + pair * 2
            w = jnp.concatenate([down_buf[slot], down_buf[slot + 1]], axis=1)
            value = jnp.dot(hidden_buf[...], w, preferred_element_type=F32)
            store_part(value, pl.ds(starts[r] + pair * 256, 256), 256)
        pair_copy(r).start()

    def finish(r, dz):
        columns = pl.ds(pl.multiple_of(lax.rem(z - dz + 4, 4) * 512, 512), 512)
        out_ref[:, columns] = (upd_buf[:, columns] + last_step(r)).astype(BF16)

    rounds = tuple(enumerate(ROW_ORDER))
    for i, (r, dz) in enumerate(rounds):
        run(("row", dz))
        mixer_sums(r, dz)
        if i >= 1:
            pair_step(r - 1)
        if i >= 2:
            mid_step(r - 2)
        if i >= 3:
            finish(*rounds[i - 3])
    pair_step(3)
    mid_step(2)
    finish(*rounds[1])
    mid_step(3)
    finish(*rounds[2])
    finish(*rounds[3])

    for r in range(4):
        pair_copy(r).wait_send()
        for k in range(2):
            mid_copy(r, k).wait_send()
            last_copy(r, k).wait_send()
    for copy in sent + ow_sent + [ex_copy(n) for n in range(4)]:
        copy.wait_send()
    each_query(lambda copy: copy.wait_send())
    each_mixed(lambda copy: copy.wait_send())
    for g, ref in enumerate((up_buf.at[pl.ds(0, 1920)], down_buf.at[pl.ds(0, 15)])):
        arrived(ref, send_sem.at[g])

    @pl.when(primary)
    def _():
        arrived(kv_buf.at[pl.ds(0, 12)], kv_send.at[0])
        arrived(kv_buf, kv_send.at[1])


def local(qn, kn, vn, qb, kb, vb, offn, offb, res, on, ob, gain, up, down):
    hbm = pl.BlockSpec(memory_space=pl.ANY)
    vmem = pl.BlockSpec(memory_space=pltpu.VMEM)
    dma = pltpu.SemaphoreType.DMA
    return pl.pallas_call(
        body,
        out_shape=jax.ShapeDtypeStruct((32, 2048), BF16),
        in_specs=[hbm, hbm, hbm, hbm, hbm, hbm, vmem, vmem, hbm, hbm, hbm, vmem, hbm, hbm],
        out_specs=vmem,
        scratch_shapes=[
            pltpu.VMEM((2, KV_ROWS, 128), BF16),
            pltpu.VMEM((16, KV_ROWS, 128), BF16),
            pltpu.VMEM((2048, 1024), BF16),
            pltpu.VMEM((16, 1024, 128), BF16),
            pltpu.VMEM((8, 128, 2048), BF16),
            pltpu.VMEM((2, 256, 128), BF16),
            pltpu.VMEM((16, 32, 128), BF16),
            pltpu.VMEM((2, 512, 128), BF16),
            pltpu.VMEM((2, 512, 128), F32),
            pltpu.VMEM((512, 128), F32),
            pltpu.VMEM((256, 256), BF16),
            pltpu.VMEM((16, 32, 128), BF16),
            pltpu.VMEM((2, 8, 32, 128), BF16),
            pltpu.VMEM((32, 2048), BF16),
            pltpu.VMEM((32, 2048), F32),
            pltpu.VMEM((32, 2048), BF16),
            pltpu.VMEM((32, 2048), BF16),
            pltpu.VMEM((2, 4, 32, 2048), BF16),
            pltpu.VMEM((4, 32, 2048), BF16),
            pltpu.VMEM((4, 32, 2048), F32),
            pltpu.VMEM((2, 32, 1024), BF16),
            pltpu.VMEM((2, 32, 1024), BF16),
            pltpu.VMEM((2, 32, 2048), BF16),
            pltpu.VMEM((2, 32, 2048), BF16),
            pltpu.VMEM((32, 2048), F32),
            pltpu.VMEM((8, 32, 2048), BF16),
            pltpu.VMEM((256, 1024), BF16),
            dma((14,)),
            dma((2, 4, 16)),
            dma((2,)),
            dma((4,)),
            dma((2,)),
            dma((4, 2)),
            dma((4, 2)),
            dma((2,)),
            dma((4, 4)),
            dma((4, 2)),
            dma((16,)),
            dma((2, 4, 2)),
            dma((2, 8)),
            dma((4, 4)),
            dma((2,)),
            dma((2,)),
            dma((2, 2)),
            dma((2, 2)),
            dma((4,)),
            dma((4,)),
            dma((4,)),
            dma((4, 2)),
            dma((4, 2)),
            dma((13,)),
            dma((13,)),
            dma((4, 5)),
        ],
        compiler_params=pltpu.CompilerParams(
            collective_id=0, has_side_effects=True, vmem_limit_bytes=60 * 1024 * 1024
        ),
    )(qn, kn, vn, qb, kb, vb, offn, offb, res, on, ob, gain.reshape(1, 2048), up, down)


def solution(mesh):
    return jax.shard_map(
        local,
        mesh=mesh,
        in_specs=(
            P("sp", "tp"), P("sp", "tp"), P("sp", "tp"), P("sp", "tp"), P("sp", "tp"), P("sp", "tp"),
            P("tp", "sp"), P("tp", "sp"), P(("sp", "tp"), None), P("tp", None), P("tp", None), P(),
            P("sp", "tp"), P("tp", "sp"),
        ),
        out_specs=P(("sp", "tp"), None),
        check_vma=False,
    )
```

time: 94.6 us -> 88.8 us (0.939)
  Pallas kernels: 92.9 us -> 86.7 us
    pallas_call x1, Pallas kernels: 92.9 us -> 86.7 us  [local(): pl.pallas_call(body, out_shape=jax.ShapeDtypeStruct((32, 2048), BF16), in...]
where the time goes in v3:
time: 88.8 us; the launch traced here: 88.3 us
  Pallas kernels  86.7 us (98%)
  local copies, waits for them, and re-layouts  1.57 us (2%)
    pallas_call x1, Pallas kernels, local(): pl.pallas_call(body, out_shape=jax.ShapeDtypeStruct((32, 2048), BF16), in...  86.7 us

profile of v3, /device:TPU:0, one launch (start us, length us, event | category | flops | bytes accessed | tf_op | source)
XLA Modules:
  0.0 88.3 jit_solution(17401871541779610027)
XLA Ops:
  0.0 86.7 %shard_map.136 = bf16[32,2048]{1,0:T(8,128)(2,1)} custom-call(bf16[256,128]{1,0:T(8,128)(2,1)} %qn_hbm.1, bf16[256,128]{1,0:T(8,128)(2,1)} %kn_hbm.1, bf16[256,128]{1,0:T(8,128)(2,1)} %vn_hbm.1, bf16[256,128]{1,0:T(8,128)(2,1)} %qb_hbm.1, bf16[256,128]{1,0:T(8,128)(2,1)} %kb_hbm.1, bf16[256,128]{1,0:T(8,128)(2,1)} %vb_hbm.1, bf16[2,256]{1,0:T(2,128)(2,1)} %offn_ref.1, ...), custom_call_target="tpu_custom_call" | custom-call | tf_op jit(solution)/shard_map/pallas_call | solution.py:708
  86.7 1.6 %copy.16 = bf16[32,2048]{1,0:T(8,128)(2,1)} copy(bf16[32,2048]{1,0:T(8,128)(2,1)} %shard_map.136) | data formatting | bytes 262144

commit v4 on v3

--- a/solution.py
+++ b/solution.py
@@ -43,19 +43,18 @@
 WIRE, DELAY = 6.0, 2.2
 POINTS = (
     ("sides", 2.8, 10.0),
-    ("keys1", 12.5, 19.0),
-    ("keys2", 17.5, 23.0),
-    ("att1", 22.0, 25.5),
-    ("att2", 24.5, 26.5),
-    ("mix1", 28.3, 33.0),
-    ("mix2", 30.0, 36.0),
-    ("mix3", 35.0, 41.0),
-    ("rows0", 38.5, 43.0),
-    ("rows1", 42.0, 46.0),
-    ("rows2", 43.5, 50.0),
+    ("keys1", 13.5, 18.0),
+    ("keys2", 17.0, 20.5),
+    ("att1", 20.3, 22.5),
+    ("mix1", 24.0, 29.0),
+    ("mix2", 26.0, 32.0),
+    ("mix3", 31.0, 37.0),
+    ("rows0", 34.0, 39.0),
+    ("rows1", 37.5, 42.0),
+    ("rows2", 39.0, 46.0),
 )
-SIZES = ((16, 16, 48, 48), (240, 240, 272, 272))
-STARTS = ((0, 16, 32, 80), (0, 240, 480, 752))
+SIZES = ((16, 16, 48, 48), (272, 272, 240, 240))
+STARTS = ((0, 16, 32, 80), (0, 272, 544, 784))
 
 
 def plan():
@@ -92,7 +91,7 @@
                 offer(g, q, child)
     for point, now, until in POINTS:
         out = []
-        axes = ("x",) if point in ("sides", "keys1") else ("x", "z")
+        axes = ("x",) if point == "sides" else ("x", "z")
         for when, event in sorted((when, event) for event, when in landing.items()):
             if when <= now - 0.3:
                 take(out, event)
@@ -122,11 +121,11 @@
     qn_hbm, kn_hbm, vn_hbm, qb_hbm, kb_hbm, vb_hbm, offn_ref, offb_ref, res_hbm,
     on_hbm, ob_hbm, gain_ref, up_hbm, down_hbm, out_ref,
     stage, kv_buf, up_buf, down_buf, outw, q_own, q_all, head_buf, kept_buf, acc_buf, tri_buf,
-    mix_out, mix_all, res_buf, att_buf, ex_out, ex_in, part_buf, pair_buf, sum_buf, mid_in, mid_out, last_out, last_in,
+    mix_out, mix_all, res_buf, att_buf, ex_out, ex_in, part_buf, pair_buf, last_out, last_in,
     upd_buf, norm_buf, hidden_buf,
     load_sem, recv_sem, send_sem, x_sem, x_send, z_sem, far_sem, kv_send, kvp_sem, kvf_sem,
     q_sem, q_send, m_sem, m_send, ow_sem, ow_send, owp_sem, owp_send, ex_sem, ex_send,
-    pair_sem, mid_sem, last_sem, row_sem, row_send, y_send,
+    pair_sem, last_sem, row_sem, row_send, y_send,
 ):
     s = lax.axis_index("sp")
     t = lax.axis_index("tp")
@@ -158,6 +157,7 @@
         "pair": {"sp": s, "tp": y * 2 + (1 - c)},
         ("y", 1): {"sp": s, "tp": y_at(1) * 2 + c},
         ("y", -1): {"sp": s, "tp": y_at(-1) * 2 + c},
+        ("y", 2): {"sp": s, "tp": y_at(2) * 2 + c},
     }
 
     def remote(src, dst, send, recv, target):
@@ -242,8 +242,10 @@
     later = lax.broadcasted_iota(jnp.int32, (256, 256), 0)
     earlier = lax.broadcasted_iota(jnp.int32, (256, 256), 1)
     tri_buf[...] = jnp.where(later >= earlier, 1.0, 0.0).astype(BF16)
+    acc_buf[...] = jnp.zeros_like(acc_buf)
+    kept_buf[...] = jnp.zeros_like(kept_buf)
     one, none = jnp.int32(1), jnp.int32(0)
-    pl.semaphore_wait(barrier, 39 - jnp.where(primary, one, none) - jnp.where(holds_own, one, none))
+    pl.semaphore_wait(barrier, 40 - jnp.where(primary, one, none) - jnp.where(holds_own, one, none))
 
     def piece(g, slot, q):
         if g == 0:
@@ -369,48 +371,11 @@
         pl.when(x != c + 2 * unit)(lambda: x_copy(unit).wait_send())
     run("sides")
 
-    @pl.when(primary)
-    def _():
-        for d in (1, 3):
-            arrived(kv_buf.at[kv_slot(d, 0)], x_sem.at[d])
-            to_column(d)
-        from_row(0)
-        arrived(kv_buf.at[kv_slot(2, 0)], x_sem.at[2])
-        to_column(2)
-        from_row(1)
-        from_row(3)
-
-    run("keys1")
-
-    @pl.when(primary)
-    def _():
-        from_row(2)
-        for d in (0, 1, 3, 2):
-            from_far(d)
-
-    @pl.when(jnp.logical_not(primary))
-    def _():
-        for d in (0, 1, 3, 2):
-            for dz in (0, 1, 3):
-                arrived(kv_buf.at[kv_slot(d, dz)], kvp_sem.at[d, dz])
-            for k in range(2):
-                arrived(far_half(d, k), kvf_sem.at[d, k])
-
-    for slot in range(16):
-        pl.when(jnp.logical_not(jnp.logical_and(primary, s == slot)))(
-            lambda: arrived(q_all.at[slot], q_sem.at[slot])
-        )
-    ow_pass(0)
-    run("keys2")
-
     lane = lax.broadcasted_iota(jnp.int32, (512, 128), 1)
     zero = jnp.zeros((), BF16)
-    acc_buf[...] = jnp.zeros_like(acc_buf)
-    kept_buf[...] = jnp.zeros_like(kept_buf)
-    queries = q_all[...].reshape(512, 128)
     ahead = (later // 32) * 256 + lax.rem(later, 32) - earlier + part * 32
 
-    def attend(slot, heads, chunks, scale):
+    def attend(slot, zz, heads, chunks, scale):
         offs = kv_buf[slot, OFF:VAL, :].astype(F32) * LOG2E
         k = kv_buf[slot, pl.ds(0, 256), :]
         v = kv_buf[slot, pl.ds(VAL, 256), :]
@@ -430,52 +395,107 @@
             gone.append(jnp.dot(drop.astype(BF16), tri_buf[...], preferred_element_type=F32))
         for (chunk, masked, h), score, lost in zip(items, scores, gone):
             rows = slice(chunk * 256, chunk * 256 + 256)
-            kept = kept_buf[h, rows]
+            kept = kept_buf[zz, h, rows]
             weight = lax.exp2(score - lost - jnp.concatenate([kept, kept], axis=1))
             if masked:
                 weight = jnp.where(ahead > slot * 256 - chunk * 2048, weight, 0.0)
-            kept_buf[h, rows] = kept + jnp.broadcast_to(lost[:, 0:1], (256, 128))
+            kept_buf[zz, h, rows] = kept + jnp.broadcast_to(lost[:, 0:1], (256, 128))
             weights.append(weight.astype(BF16))
         for chunk, _ in chunks:
             rows = slice(chunk * 256, chunk * 256 + 256)
-            total = acc_buf[rows]
+            total = acc_buf[zz, rows]
             for (other, _, h), weight in zip(items, weights):
                 if other == chunk:
                     values = v
                     if heads == 2:
                         values = jnp.where((lane[:256] < 64) if h == 0 else (lane[:256] >= 64), v, zero)
                     total = total + jnp.dot(weight, values, preferred_element_type=F32)
-            acc_buf[rows] = total
-
-    def attention(heads, scale):
+            acc_buf[zz, rows] = total
+
+    def each_group(act):
+        pl.when(x < 2)(lambda: act(2, LOG2E * 64**-0.5))
+        pl.when(x >= 2)(lambda: act(1, LOG2E * 128**-0.5))
+
+    def set_heads(heads, scale):
+        queries = q_all[...].reshape(512, 128)
         if heads == 2:
             head_buf[0] = jnp.where(lane < 64, queries, zero)
             head_buf[1] = jnp.where(lane >= 64, queries, zero)
         else:
             head_buf[0] = queries
 
-    def each_group(act):
-        pl.when(x < 2)(lambda: act(2, LOG2E * 64**-0.5))
-        pl.when(x >= 2)(lambda: act(1, LOG2E * 128**-0.5))
-
-    def late_keys(heads, scale):
-        if heads == 2:
-            head_buf[0] = jnp.where(lane < 64, queries, zero)
-            head_buf[1] = jnp.where(lane >= 64, queries, zero)
-        else:
-            head_buf[0] = queries
-        pl.loop(0, 8)(lambda k: attend(15 - k, heads, ((1, True),), scale))
-
-    def early_keys(first, heads, scale):
-        pl.loop(0, 4)(lambda k: attend(first - k, heads, ((0, True), (1, False)), scale))
-
-    each_group(late_keys)
+    def attend_row(dz):
+        zz = z_at(-dz)
+
+        def act(heads, scale):
+            for near, chunks in ((True, ((1, True),)), (False, ((0, True), (1, False)))):
+
+                @pl.when((zz >= 2) if near else (zz < 2))
+                def _():
+                    pl.loop(0, 4)(lambda k: attend(zz * 4 + 3 - k, zz, heads, chunks, scale))
+
+        each_group(act)
+
+    def join_rows(heads, scale):
+        total, past = acc_buf[3], None
+        for zz in (2, 1, 0):
+            kept = kept_buf[zz + 1, 0]
+            if heads == 2:
+                kept = jnp.where(lane < 64, kept, kept_buf[zz + 1, 1])
+            past = kept if past is None else past + kept
+            total = total + acc_buf[zz] * lax.exp2(-past)
+        mix_out[...] = total.reshape(16, 32, 128).astype(BF16)
+
+    def secondary_waits(rows):
+        @pl.when(jnp.logical_not(primary))
+        def _():
+            for d in (0, 1, 3, 2):
+                for dz in rows:
+                    if dz == 2:
+                        for k in range(2):
+                            arrived(far_half(d, k), kvf_sem.at[d, k])
+                    else:
+                        arrived(kv_buf.at[kv_slot(d, dz)], kvp_sem.at[d, dz])
+
+    @pl.when(primary)
+    def _():
+        for d in (1, 3):
+            arrived(kv_buf.at[kv_slot(d, 0)], x_sem.at[d])
+            to_column(d)
+        from_row(0)
+        arrived(kv_buf.at[kv_slot(2, 0)], x_sem.at[2])
+        to_column(2)
+
+    for slot in range(16):
+        pl.when(jnp.logical_not(jnp.logical_and(primary, s == slot)))(
+            lambda: arrived(q_all.at[slot], q_sem.at[slot])
+        )
+    each_group(set_heads)
+    secondary_waits((0,))
+    attend_row(0)
+
+    @pl.when(primary)
+    def _():
+        from_row(1)
+        from_row(3)
+        from_row(2)
+
+    run("keys1")
+    secondary_waits((1, 3))
+    attend_row(1)
+    ow_pass(0)
+
+    @pl.when(primary)
+    def _():
+        for d in (0, 1, 3, 2):
+            from_far(d)
+
+    run("keys2")
+    attend_row(3)
     run("att1")
-    each_group(functools.partial(early_keys, 7))
-    run("att2")
-    each_group(functools.partial(early_keys, 3))
-
-    mix_out[...] = acc_buf[...].reshape(16, 32, 128).astype(BF16)
+    secondary_waits((2,))
+    attend_row(2)
+    each_group(join_rows)
 
     def m_copy(dx, dz):
         return remote(
@@ -583,35 +603,19 @@
         pre = jnp.maximum(jnp.dot(rows, up_buf[:, columns], preferred_element_type=F32), 0.0)
         hidden_buf[:, columns] = (pre * pre).astype(BF16)
 
-    widths = (512, 512, 512, 512)
-    starts = (0, 512, 1024, 1536)
-
-    def cols(r, lo=0, hi=None):
-        hi = widths[r] if hi is None else hi
-        return pl.ds(starts[r] + lo, hi - lo)
-
-    def half_cols(r, k=0):
-        return pl.ds(starts[r] // 2, widths[r] // 2)
+    def cols(r):
+        return pl.ds(r * 512, 512)
 
     def pair_copy(r):
-        return pltpu.make_async_remote_copy(
-            src_ref=part_buf.at[1 - c, :, :, cols(r)], dst_ref=pair_buf.at[:, :, cols(r)],
-            send_sem=y_send.at[r, 0], recv_sem=pair_sem.at[r],
-            device_id=neighbour["pair"], device_id_type=MESH,
+        return remote(
+            part_buf.at[1 - c, :, :, cols(r)], pair_buf.at[:, :, cols(r)], y_send.at[r, 3], pair_sem.at[r],
+            neighbour["pair"],
         )
 
-    def mid_copy(r, k):
-        return pltpu.make_async_remote_copy(
-            src_ref=mid_out.at[k, :, half_cols(r)], dst_ref=mid_in.at[k, :, half_cols(r)],
-            send_sem=y_send.at[r, 1 + k], recv_sem=mid_sem.at[r, k],
-            device_id=neighbour["y", 1 if k == 0 else -1], device_id_type=MESH,
-        )
-
     def last_copy(r, k):
-        return pltpu.make_async_remote_copy(
-            src_ref=last_out.at[k, :, cols(r)], dst_ref=last_in.at[k, :, cols(r)],
-            send_sem=y_send.at[r, 3 + k], recv_sem=last_sem.at[r, k],
-            device_id=neighbour["y", 1 if k == 0 else -1], device_id_type=MESH,
+        return remote(
+            last_out.at[k, :, cols(r)], last_in.at[k, :, cols(r)], y_send.at[r, k], last_sem.at[r, k],
+            neighbour["y", (2, 1, -1)[k]],
         )
 
     def store_part(value, columns, width):
@@ -620,38 +624,22 @@
             for yy in range(4):
                 part_buf[core, yy, :, columns] = blocks[yy, core].astype(BF16)
 
+    def pair_sum(r, dy):
+        yy = y_at(dy)
+        return part_buf[c, yy, :, cols(r)].astype(F32) + pair_buf[yy, :, cols(r)].astype(F32)
+
     def pair_step(r):
         pair_copy(r).wait_recv()
-        half = widths[r] // 2
-        for yy in range(4):
-            sum_buf[yy, :, cols(r)] = (
-                part_buf[c, yy, :, cols(r)].astype(F32) + pair_buf[yy, :, cols(r)].astype(F32)
-            )
-        far = y_at(2)
-        mid_out[0, :, half_cols(r)] = sum_buf[far, :, cols(r, 0, half)].astype(BF16)
-        mid_out[1, :, half_cols(r)] = sum_buf[far, :, cols(r, half)].astype(BF16)
-        mid_copy(r, 0).start()
-        mid_copy(r, 1).start()
-
-    def mid_step(r):
-        half = widths[r] // 2
-        for k, dy in ((0, 1), (1, -1)):
-            to = y_at(dy)
-            mid_copy(r, k).wait_recv()
-            left = sum_buf[to, :, cols(r, 0, half)]
-            right = sum_buf[to, :, cols(r, half)]
-            passing = mid_in[k, :, half_cols(r)].astype(F32)
-            left, right = (left + passing, right) if k == 0 else (left, right + passing)
-            last_out[k, :, cols(r, 0, half)] = left.astype(BF16)
-            last_out[k, :, cols(r, half)] = right.astype(BF16)
+        for k, dy in enumerate((2, 1, -1)):
+            last_out[k, :, cols(r)] = pair_sum(r, dy).astype(BF16)
             last_copy(r, k).start()
 
     def last_step(r):
-        last_copy(r, 0).wait_recv()
-        last_copy(r, 1).wait_recv()
-        return (
-            sum_buf[y, :, cols(r)] + last_in[0, :, cols(r)].astype(F32) + last_in[1, :, cols(r)].astype(F32)
-        )
+        total = pair_sum(r, 0)
+        for k in range(3):
+            last_copy(r, k).wait_recv()
+            total = total + last_in[k, :, cols(r)].astype(F32)
+        return total
 
     def mixer_sums(r, dz):
         zz = lax.rem(z - dz + 4, 4)
@@ -659,7 +647,7 @@
             slot = zz * 4 + pair * 2
             w = jnp.concatenate([down_buf[slot], down_buf[slot + 1]], axis=1)
             value = jnp.dot(hidden_buf[...], w, preferred_element_type=F32)
-            store_part(value, pl.ds(starts[r] + pair * 256, 256), 256)
+            store_part(value, pl.ds(r * 512 + pair * 256, 256), 256)
         pair_copy(r).start()
 
     def finish(r, dz):
@@ -672,21 +660,15 @@
         mixer_sums(r, dz)
         if i >= 1:
             pair_step(r - 1)
-        if i >= 2:
-            mid_step(r - 2)
         if i >= 3:
             finish(*rounds[i - 3])
     pair_step(3)
-    mid_step(2)
-    finish(*rounds[1])
-    mid_step(3)
-    finish(*rounds[2])
-    finish(*rounds[3])
+    for r, dz in rounds[1:]:
+        finish(r, dz)
 
     for r in range(4):
         pair_copy(r).wait_send()
-        for k in range(2):
-            mid_copy(r, k).wait_send()
+        for k in range(3):
             last_copy(r, k).wait_send()
     for copy in sent + ow_sent + [ex_copy(n) for n in range(4)]:
         copy.wait_send()
@@ -719,8 +701,8 @@
             pltpu.VMEM((2, 256, 128), BF16),
             pltpu.VMEM((16, 32, 128), BF16),
             pltpu.VMEM((2, 512, 128), BF16),
-            pltpu.VMEM((2, 512, 128), F32),
-            pltpu.VMEM((512, 128), F32),
+            pltpu.VMEM((4, 2, 512, 128), F32),
+            pltpu.VMEM((4, 512, 128), F32),
             pltpu.VMEM((256, 256), BF16),
             pltpu.VMEM((16, 32, 128), BF16),
             pltpu.VMEM((2, 8, 32, 128), BF16),
@@ -730,11 +712,8 @@
             pltpu.VMEM((32, 2048), BF16),
             pltpu.VMEM((2, 4, 32, 2048), BF16),
             pltpu.VMEM((4, 32, 2048), BF16),
-            pltpu.VMEM((4, 32, 2048), F32),
-            pltpu.VMEM((2, 32, 1024), BF16),
-            pltpu.VMEM((2, 32, 1024), BF16),
-            pltpu.VMEM((2, 32, 2048), BF16),
-            pltpu.VMEM((2, 32, 2048), BF16),
+            pltpu.VMEM((3, 32, 2048), BF16),
+            pltpu.VMEM((3, 32, 2048), BF16),
             pltpu.VMEM((32, 2048), F32),
             pltpu.VMEM((8, 32, 2048), BF16),
             pltpu.VMEM((256, 1024), BF16),
@@ -759,11 +738,10 @@
             dma((4,)),
             dma((4,)),
             dma((4,)),
-            dma((4, 2)),
-            dma((4, 2)),
+            dma((4, 3)),
             dma((13,)),
             dma((13,)),
-            dma((4, 5)),
+            dma((4, 4)),
         ],
         compiler_params=pltpu.CompilerParams(
             collective_id=0, has_side_effects=True, vmem_limit_bytes=60 * 1024 * 1024

time: 88.8 us -> 81.6 us (0.919)
  Pallas kernels: 86.7 us -> 79.3 us
    pallas_call x1, Pallas kernels: 86.7 us -> 79.3 us  [local(): pl.pallas_call(body, out_shape=jax.ShapeDtypeStruct((32, 2048), BF16), in...]
where the time goes in v4:
time: 81.6 us; the launch traced here: 80.9 us
  Pallas kernels  79.3 us (97%)
  local copies, waits for them, and re-layouts  1.57 us (2%)
    pallas_call x1, Pallas kernels, local(): pl.pallas_call(body, out_shape=jax.ShapeDtypeStruct((32, 2048), BF16), in...  79.3 us

profile of v4, /device:TPU:0, one launch (start us, length us, event | category | flops | bytes accessed | tf_op | source)
XLA Modules:
  0.0 80.9 jit_solution(10543956404074696940)
XLA Ops:
  0.0 79.3 %shard_map.136 = bf16[32,2048]{1,0:T(8,128)(2,1)} custom-call(bf16[256,128]{1,0:T(8,128)(2,1)} %qn_hbm.1, bf16[256,128]{1,0:T(8,128)(2,1)} %kn_hbm.1, bf16[256,128]{1,0:T(8,128)(2,1)} %vn_hbm.1, bf16[256,128]{1,0:T(8,128)(2,1)} %qb_hbm.1, bf16[256,128]{1,0:T(8,128)(2,1)} %kb_hbm.1, bf16[256,128]{1,0:T(8,128)(2,1)} %vb_hbm.1, bf16[2,256]{1,0:T(2,128)(2,1)} %offn_ref.1, ...), custom_call_target="tpu_custom_call" | custom-call | tf_op jit(solution)/shard_map/pallas_call | solution.py:690
  79.4 1.6 %copy.16 = bf16[32,2048]{1,0:T(8,128)(2,1)} copy(bf16[32,2048]{1,0:T(8,128)(2,1)} %shard_map.136) | data formatting | bytes 262144

commit v5 on v4

--- a/solution.py
+++ b/solution.py
@@ -42,16 +42,16 @@
 
 WIRE, DELAY = 6.0, 2.2
 POINTS = (
-    ("sides", 2.8, 10.0),
-    ("keys1", 13.5, 18.0),
-    ("keys2", 17.0, 20.5),
-    ("att1", 20.3, 22.5),
-    ("mix1", 24.0, 29.0),
-    ("mix2", 26.0, 32.0),
-    ("mix3", 31.0, 37.0),
-    ("rows0", 34.0, 39.0),
-    ("rows1", 37.5, 42.0),
-    ("rows2", 39.0, 46.0),
+    ("sides", 2.8, 14.0),
+    ("keys1", 15.5, 20.0),
+    ("keys2", 19.0, 22.5),
+    ("att1", 22.3, 24.5),
+    ("mix1", 26.0, 31.0),
+    ("mix2", 28.0, 34.0),
+    ("mix3", 33.0, 39.0),
+    ("rows0", 36.0, 41.0),
+    ("rows1", 39.5, 44.0),
+    ("rows2", 41.0, 48.0),
 )
 SIZES = ((16, 16, 48, 48), (272, 272, 240, 240))
 STARTS = ((0, 16, 32, 80), (0, 272, 544, 784))
@@ -119,13 +119,12 @@
 
 def body(
     qn_hbm, kn_hbm, vn_hbm, qb_hbm, kb_hbm, vb_hbm, offn_ref, offb_ref, res_hbm,
-    on_hbm, ob_hbm, gain_ref, up_hbm, down_hbm, out_ref,
+    on_hbm, ob_hbm, gain_ref, up_hbm, down_hbm, out_hbm,
     stage, kv_buf, up_buf, down_buf, outw, q_own, q_all, head_buf, kept_buf, acc_buf, tri_buf,
     mix_out, mix_all, res_buf, att_buf, ex_out, ex_in, part_buf, pair_buf, last_out, last_in,
-    upd_buf, norm_buf, hidden_buf,
-    load_sem, recv_sem, send_sem, x_sem, x_send, z_sem, far_sem, kv_send, kvp_sem, kvf_sem,
-    q_sem, q_send, m_sem, m_send, ow_sem, ow_send, owp_sem, owp_send, ex_sem, ex_send,
-    pair_sem, last_sem, row_sem, row_send, y_send,
+    upd_buf, norm_buf, hidden_buf, out_buf,
+    load_sem, recv_sem, send_sem, x_sem, x_send, z_sem, far_sem, kv_send, kvp_sem,
+    q_sem, m_sem, ow_sem, ex_sem, pair_sem, last_sem, row_sem, y_send, out_sem,
 ):
     s = lax.axis_index("sp")
     t = lax.axis_index("tp")
@@ -182,15 +181,16 @@
         (down_hbm, down_buf.at[s]),
         (res_hbm, res_buf),
     ]
-    loads = [pltpu.make_async_copy(a, b, load_sem.at[k]) for k, (a, b) in enumerate(loads)]
+    groups = (0, 0, 0, 0, 1, 1, 2, 2, 3, 3, 4)
+    loads = [pltpu.make_async_copy(a, b, load_sem.at[k]) for k, (a, b) in zip(groups, loads)]
     for copy in loads:
         copy.start()
 
     mine = [
         [
-            pltpu.make_async_copy(k_hbm, kv_buf.at[s, pl.ds(0, 256)], load_sem.at[11]),
-            pltpu.make_async_copy(v_hbm, kv_buf.at[s, pl.ds(VAL, 256)], load_sem.at[12]),
-            pltpu.make_async_copy(q_hbm.at[pl.ds(pl.multiple_of(part * 32, 32), 32)], q_all.at[s], load_sem.at[13]),
+            pltpu.make_async_copy(k_hbm, kv_buf.at[s, pl.ds(0, 256)], load_sem.at[5]),
+            pltpu.make_async_copy(v_hbm, kv_buf.at[s, pl.ds(VAL, 256)], load_sem.at[5]),
+            pltpu.make_async_copy(q_hbm.at[pl.ds(pl.multiple_of(part * 32, 32), 32)], q_all.at[s], load_sem.at[6]),
         ]
         for k_hbm, v_hbm, q_hbm in ((kn_hbm, vn_hbm, qn_hbm), (kb_hbm, vb_hbm, qb_hbm))
     ]
@@ -266,8 +266,7 @@
                 dx, dz = what
                 arrived(piece(g, xz(-dx, -dz), q), recv_sem.at[g, q, dz * 4 + dx])
 
-    for copy in loads[:4]:
-        copy.wait()
+    arrived(head_buf, load_sem.at[0])
 
     def x_copy(unit):
         col = c + 2 * unit
@@ -289,7 +288,7 @@
         ref = kv_buf.at[kv_slot(d, 0)]
         remote(ref, ref, kv_send.at[0], z_sem.at[d, 0], neighbour["z", 1]).start()
         remote(ref, ref, kv_send.at[0], z_sem.at[d, 1], neighbour["z", -1]).start()
-        remote(ref, ref, kv_send.at[1], kvp_sem.at[d, 0], neighbour["pair"]).start()
+        remote(ref, ref, kv_send.at[1], kvp_sem.at[0], neighbour["pair"]).start()
 
     def from_row(d):
         for k, dz in ((0, 1), (1, 3)):
@@ -298,7 +297,7 @@
             arrived(ref, z_sem.at[d, k])
             half = kv_buf.at[slot, pl.ds(0, VAL) if k == 0 else pl.ds(VAL, 256)]
             remote(half, half, kv_send.at[0], far_sem.at[d, k], neighbour["z", 1 if k == 0 else -1]).start()
-            remote(ref, ref, kv_send.at[1], kvp_sem.at[d, dz], neighbour["pair"]).start()
+            remote(ref, ref, kv_send.at[1], kvp_sem.at[dz], neighbour["pair"]).start()
 
     def far_half(d, k):
         return kv_buf.at[kv_slot(d, 2), pl.ds(0, VAL) if k == 0 else pl.ds(VAL, 256)]
@@ -307,27 +306,22 @@
         for k in range(2):
             half = far_half(d, k)
             arrived(half, far_sem.at[d, k])
-            remote(half, half, kv_send.at[1], kvf_sem.at[d, k], neighbour["pair"]).start()
+            remote(half, half, kv_send.at[1], kvp_sem.at[2], neighbour["pair"]).start()
 
     @pl.when(primary)
     def _():
-        for unit in range(2):
-
-            @pl.when(x == c + 2 * unit)
-            def _():
-                for copy in mine[unit]:
-                    copy.wait()
-
+        arrived(q_own, load_sem.at[5])
+        arrived(q_all.at[s], load_sem.at[6])
         to_column(0)
 
-    for copy in loads[4:8]:
-        copy.wait()
+    arrived(q_own, load_sem.at[1])
+    arrived(outw.at[pl.ds(0, 2)], load_sem.at[2])
 
     def q_copy(unit, dz, dc):
         core = c if dc == 0 else 1 - c
         rows = pl.ds(pl.multiple_of((z_at(dz) * 2 + core) * 32, 32), 32)
         return remote(
-            q_own.at[unit, rows], q_all.at[s], q_send.at[unit, dz, dc], q_sem.at[s],
+            q_own.at[unit, rows], q_all.at[s], q_sem.at[0], q_sem.at[1],
             {"sp": z_at(dz) * 4 + c + 2 * unit, "tp": y * 2 + core},
         )
 
@@ -349,24 +343,20 @@
     mate = {"sp": s, "tp": y_mate * 2 + c}
 
     def ow_copy(k):
-        return remote(ow(k, 0, c), ow(k, 0, c), ow_send.at[k], ow_sem.at[k], mate)
+        return remote(ow(k, 0, c), ow(k, 0, c), ow_sem.at[2], ow_sem.at[k], mate)
 
     def ow_pair(k, foreign):
         ref = ow(k, foreign, c)
-        return remote(ref, ref, owp_send.at[k, foreign], owp_sem.at[k, foreign], neighbour["pair"])
-
-    ow_sent = [ow_copy(0), ow_copy(1), ow_pair(0, 0), ow_pair(1, 0)]
-    for copy in ow_sent:
+        return remote(ref, ref, ow_sem.at[3], ow_sem.at[4], neighbour["pair"])
+
+    for copy in (ow_copy(0), ow_copy(1), ow_pair(0, 0), ow_pair(1, 0)):
         copy.start()
 
     def ow_pass(k):
         arrived(ow(k, 1, c), ow_sem.at[k])
-        copy = ow_pair(k, 1)
-        copy.start()
-        ow_sent.append(copy)
-
-    loads[8].wait()
-    loads[9].wait()
+        ow_pair(k, 1).start()
+
+    arrived(outw.at[0], load_sem.at[3])
     for unit in range(2):
         pl.when(x != c + 2 * unit)(lambda: x_copy(unit).wait_send())
     run("sides")
@@ -449,13 +439,8 @@
     def secondary_waits(rows):
         @pl.when(jnp.logical_not(primary))
         def _():
-            for d in (0, 1, 3, 2):
-                for dz in rows:
-                    if dz == 2:
-                        for k in range(2):
-                            arrived(far_half(d, k), kvf_sem.at[d, k])
-                    else:
-                        arrived(kv_buf.at[kv_slot(d, dz)], kvp_sem.at[d, dz])
+            for dz in rows:
+                arrived(kv_buf.at[pl.ds(pl.multiple_of(z_at(-dz) * 4, 4), 4)], kvp_sem.at[dz])
 
     @pl.when(primary)
     def _():
@@ -466,10 +451,11 @@
         arrived(kv_buf.at[kv_slot(2, 0)], x_sem.at[2])
         to_column(2)
 
-    for slot in range(16):
-        pl.when(jnp.logical_not(jnp.logical_and(primary, s == slot)))(
-            lambda: arrived(q_all.at[slot], q_sem.at[slot])
-        )
+    def all_but(mine, ref, sem):
+        pl.when(mine)(lambda: arrived(ref.at[pl.ds(0, 15)], sem))
+        pl.when(jnp.logical_not(mine))(lambda: arrived(ref, sem))
+
+    all_but(primary, q_all, q_sem.at[1])
     each_group(set_heads)
     secondary_waits((0,))
     attend_row(0)
@@ -499,8 +485,8 @@
 
     def m_copy(dx, dz):
         return remote(
-            mix_out.at[xz(dx, dz)], mix_all.at[mix_block, y_odd * 4 + x], m_send.at[dz, dx],
-            m_sem.at[mix_block, y_odd * 4 + x], {"sp": xz(dx, dz), "tp": mix_y * 2 + c},
+            mix_out.at[xz(dx, dz)], mix_all.at[mix_block, y_odd * 4 + x], m_sem.at[0],
+            m_sem.at[1], {"sp": xz(dx, dz), "tp": mix_y * 2 + c},
         )
 
     def each_mixed(act):
@@ -520,23 +506,16 @@
     run("mix1")
     ow_pass(1)
     run("mix2")
-    for block in range(2):
-        for unit in range(8):
-            from_me = jnp.logical_and(holds_own, jnp.logical_and(mix_block == block, y_odd * 4 + x == unit))
-            pl.when(jnp.logical_not(from_me))(
-                lambda: arrived(mix_all.at[block, unit], m_sem.at[block, unit])
-            )
-    for k in range(2):
-        for foreign in range(2):
-            arrived(ow(k, foreign, 1 - c), owp_sem.at[k, foreign])
-    loads[10].wait()
+    all_but(holds_own, mix_out, m_sem.at[1])
+    arrived(outw.at[pl.ds(0, 4)], ow_sem.at[4])
+    arrived(res_buf, load_sem.at[4])
 
     mixed = jnp.concatenate([mix_all[:, unit].reshape(64, 128) for unit in range(8)], axis=1)
 
     def ex_copy(n):
         columns = pl.ds(n * 512, 512)
         return remote(
-            ex_out.at[:, columns], ex_in.at[:, columns], ex_send.at[n], ex_sem.at[n],
+            ex_out.at[:, columns], ex_in.at[:, columns], ex_sem.at[0], ex_sem.at[1],
             {"sp": s, "tp": (3 - y) * 2 + c},
         )
 
@@ -547,26 +526,21 @@
         ex_out[:, columns] = sums[32:].astype(BF16)
         ex_copy(n).start()
     run("mix3")
-    for n in range(4):
-        ex_copy(n).wait_recv()
+    arrived(ex_in, ex_sem.at[1])
     updated = res_buf[...].astype(F32) + (att_buf[...] + ex_in[...].astype(F32))
     upd_buf[...] = updated
     scale = lax.rsqrt(jnp.mean(updated * updated, axis=-1, keepdims=True) + 1e-06)
     norm_buf[t] = (updated * scale * gain_ref[...]).astype(BF16)
 
     def row_copy(ref, target, k):
-        return remote(ref, ref, row_send.at[k], row_sem.at[k], neighbour[target])
+        return remote(ref, ref, row_sem.at[7], row_sem.at[k if k < 6 else 6], neighbour[target])
 
     def half_rows(dy, k, core=None):
         slot = y_at(dy) * 2 + (c if core is None else core)
         return norm_buf.at[slot, pl.ds(16 * k, 16)]
 
-    sent = []
-
     def row_send_to(ref, target, k):
-        copy = row_copy(ref, target, k)
-        copy.start()
-        sent.append(copy)
+        row_copy(ref, target, k).start()
 
     row_send_to(half_rows(0, 0), ("y", 1), 0)
     row_send_to(half_rows(0, 1), ("y", -1), 1)
@@ -590,11 +564,7 @@
     row_send_to(half_rows(2, 0), "pair", 11)
     arrived(half_rows(2, 1), row_sem.at[5])
     row_send_to(half_rows(2, 1), "pair", 12)
-    other = 1 - c
-    arrived(norm_buf.at[y * 2 + other], row_sem.at[6])
-    for k, (dy, half) in enumerate(((-1, 0), (1, 1), (-1, 1), (1, 0), (2, 0), (2, 1))):
-        arrived(half_rows(dy, half, other), row_sem.at[7 + k])
-
+    arrived(norm_buf.at[pl.ds(0, 4)], row_sem.at[6])
     run("up")
     @pl.loop(0, 4)
     def _(n):
@@ -608,13 +578,13 @@
 
     def pair_copy(r):
         return remote(
-            part_buf.at[1 - c, :, :, cols(r)], pair_buf.at[:, :, cols(r)], y_send.at[r, 3], pair_sem.at[r],
+            part_buf.at[1 - c, :, :, cols(r)], pair_buf.at[:, :, cols(r)], y_send.at[0], pair_sem.at[r],
             neighbour["pair"],
         )
 
     def last_copy(r, k):
         return remote(
-            last_out.at[k, :, cols(r)], last_in.at[k, :, cols(r)], y_send.at[r, k], last_sem.at[r, k],
+            last_out.at[k, :, cols(r)], last_in.at[k, :, cols(r)], y_send.at[1], last_sem.at[r],
             neighbour["y", (2, 1, -1)[k]],
         )
 
@@ -636,8 +606,8 @@
 
     def last_step(r):
         total = pair_sum(r, 0)
+        arrived(last_in.at[:, :, cols(r)], last_sem.at[r])
         for k in range(3):
-            last_copy(r, k).wait_recv()
             total = total + last_in[k, :, cols(r)].astype(F32)
         return total
 
@@ -652,7 +622,8 @@
 
     def finish(r, dz):
         columns = pl.ds(pl.multiple_of(lax.rem(z - dz + 4, 4) * 512, 512), 512)
-        out_ref[:, columns] = (upd_buf[:, columns] + last_step(r)).astype(BF16)
+        out_buf[:, columns] = (upd_buf[:, columns] + last_step(r)).astype(BF16)
+        pltpu.make_async_copy(out_buf.at[:, columns], out_hbm.at[:, columns], out_sem.at[0]).start()
 
     rounds = tuple(enumerate(ROW_ORDER))
     for i, (r, dz) in enumerate(rounds):
@@ -660,20 +631,18 @@
         mixer_sums(r, dz)
         if i >= 1:
             pair_step(r - 1)
-        if i >= 3:
-            finish(*rounds[i - 3])
     pair_step(3)
-    for r, dz in rounds[1:]:
+    for r, dz in rounds:
         finish(r, dz)
 
-    for r in range(4):
-        pair_copy(r).wait_send()
-        for k in range(3):
-            last_copy(r, k).wait_send()
-    for copy in sent + ow_sent + [ex_copy(n) for n in range(4)]:
-        copy.wait_send()
-    each_query(lambda copy: copy.wait_send())
-    each_mixed(lambda copy: copy.wait_send())
+    arrived(pair_buf, y_send.at[0])
+    arrived(last_out, y_send.at[1])
+    arrived(norm_buf.at[pl.ds(0, 7)], row_sem.at[7])
+    arrived(outw.at[pl.ds(0, 2)], ow_sem.at[2])
+    arrived(outw.at[pl.ds(0, 4)], ow_sem.at[3])
+    arrived(ex_out, ex_sem.at[0])
+    all_but(primary, q_all, q_sem.at[0])
+    all_but(holds_own, mix_out, m_sem.at[0])
     for g, ref in enumerate((up_buf.at[pl.ds(0, 1920)], down_buf.at[pl.ds(0, 15)])):
         arrived(ref, send_sem.at[g])
 
@@ -681,6 +650,8 @@
     def _():
         arrived(kv_buf.at[pl.ds(0, 12)], kv_send.at[0])
         arrived(kv_buf, kv_send.at[1])
+
+    pltpu.make_async_copy(out_buf, out_hbm, out_sem.at[0]).wait()
 
 
 def local(qn, kn, vn, qb, kb, vb, offn, offb, res, on, ob, gain, up, down):
@@ -691,7 +662,7 @@
         body,
         out_shape=jax.ShapeDtypeStruct((32, 2048), BF16),
         in_specs=[hbm, hbm, hbm, hbm, hbm, hbm, vmem, vmem, hbm, hbm, hbm, vmem, hbm, hbm],
-        out_specs=vmem,
+        out_specs=hbm,
         scratch_shapes=[
             pltpu.VMEM((2, KV_ROWS, 128), BF16),
             pltpu.VMEM((16, KV_ROWS, 128), BF16),
@@ -717,7 +688,8 @@
             pltpu.VMEM((32, 2048), F32),
             pltpu.VMEM((8, 32, 2048), BF16),
             pltpu.VMEM((256, 1024), BF16),
-            dma((14,)),
+            pltpu.VMEM((32, 2048), BF16),
+            dma((7,)),
             dma((2, 4, 16)),
             dma((2,)),
             dma((4,)),
@@ -725,23 +697,16 @@
             dma((4, 2)),
             dma((4, 2)),
             dma((2,)),
-            dma((4, 4)),
-            dma((4, 2)),
-            dma((16,)),
-            dma((2, 4, 2)),
-            dma((2, 8)),
-            dma((4, 4)),
+            dma((4,)),
             dma((2,)),
             dma((2,)),
-            dma((2, 2)),
-            dma((2, 2)),
+            dma((5,)),
+            dma((2,)),
             dma((4,)),
             dma((4,)),
-            dma((4,)),
-            dma((4, 3)),
-            dma((13,)),
-            dma((13,)),
-            dma((4, 4)),
+            dma((8,)),
+            dma((2,)),
+            dma((1,)),
         ],
         compiler_params=pltpu.CompilerParams(
             collective_id=0, has_side_effects=True, vmem_limit_bytes=60 * 1024 * 1024

time: 81.6 us -> 78.9 us (0.967)
  Pallas kernels: 79.3 us -> 76.2 us
    pallas_call x1, Pallas kernels: 79.3 us -> 76.2 us  [local(): pl.pallas_call(body, out_shape=jax.ShapeDtypeStruct((32, 2048), BF16), in...]
where the time goes in v5:
time: 78.9 us; the launch traced here: 77.8 us
  Pallas kernels  76.2 us (97%)
  local copies, waits for them, and re-layouts  1.57 us (2%)
    pallas_call x1, Pallas kernels, local(): pl.pallas_call(body, out_shape=jax.ShapeDtypeStruct((32, 2048), BF16), in...  76.2 us

profile of v5, /device:TPU:0, one launch (start us, length us, event | category | flops | bytes accessed | tf_op | source)
XLA Modules:
  0.0 77.8 jit_solution(11558047605948383036)
XLA Ops:
  0.0 76.2 %shard_map.136 = bf16[32,2048]{1,0:T(8,128)(2,1)} custom-call(bf16[256,128]{1,0:T(8,128)(2,1)} %qn_hbm.1, bf16[256,128]{1,0:T(8,128)(2,1)} %kn_hbm.1, bf16[256,128]{1,0:T(8,128)(2,1)} %vn_hbm.1, bf16[256,128]{1,0:T(8,128)(2,1)} %qb_hbm.1, bf16[256,128]{1,0:T(8,128)(2,1)} %kb_hbm.1, bf16[256,128]{1,0:T(8,128)(2,1)} %vb_hbm.1, bf16[2,256]{1,0:T(2,128)(2,1)} %offn_ref.1, ...), custom_call_target="tpu_custom_call" | custom-call | tf_op jit(solution)/shard_map/pallas_call | solution.py:661
  76.3 1.6 %copy.16 = bf16[32,2048]{1,0:T(8,128)(2,1)} copy(bf16[32,2048]{1,0:T(8,128)(2,1)} %shard_map.136) | data formatting | bytes 262144

commit v6 on v5

--- a/solution.py
+++ b/solution.py
@@ -40,25 +40,27 @@
     return out
 
 
-WIRE, DELAY = 6.0, 2.2
+WIRE, DELAY = 5.4, 2.2
 POINTS = (
+    ("first", 0.3, 4.0),
     ("sides", 2.8, 14.0),
     ("keys1", 15.5, 20.0),
     ("keys2", 19.0, 22.5),
     ("att1", 22.3, 24.5),
-    ("mix1", 26.0, 31.0),
-    ("mix2", 28.0, 34.0),
-    ("mix3", 33.0, 39.0),
-    ("rows0", 36.0, 41.0),
-    ("rows1", 39.5, 44.0),
-    ("rows2", 41.0, 48.0),
+    ("mix1", 27.5, 32.5),
+    ("mix2", 29.5, 35.5),
+    ("mix3", 34.5, 40.5),
+    ("rows0", 37.5, 42.5),
+    ("rows1", 41.0, 45.5),
+    ("rows2", 42.5, 49.5),
 )
-SIZES = ((16, 16, 48, 48), (272, 272, 240, 240))
-STARTS = ((0, 16, 32, 80), (0, 272, 544, 784))
+KEYS_END = 15.0
+SIZES = ((16, 16, 48, 48), (336, 336, 176, 176))
+STARTS = ((0, 16, 32, 80), (0, 336, 672, 848))
 
 
 def plan():
-    free = {(axis, step): 0.0 for axis in "xz" for step in (1, -1)}
+    free = {(axis, step): 1.5 for axis in "xz" for step in (1, -1)}
     landing, backlog, steps = {}, [], {}
     left = {(g, dz): 12 if dz == 0 else 16 for g in range(2) for dz in range(4)}
 
@@ -91,11 +93,13 @@
                 offer(g, q, child)
     for point, now, until in POINTS:
         out = []
-        axes = ("x",) if point == "sides" else ("x", "z")
+        axes = {"first": ("z",), "sides": ("x",)}.get(point, ("x", "z"))
         for when, event in sorted((when, event) for event, when in landing.items()):
             if when <= now - 0.3:
                 take(out, event)
         issue(now, out, until, axes)
+        if point == "first":
+            free["z", 1] = free["z", -1] = KEYS_END
         steps[point] = out
     order, out = [], []
     while landing or backlog:
@@ -357,6 +361,7 @@
         ow_pair(k, 1).start()
 
     arrived(outw.at[0], load_sem.at[3])
+    run("first")
     for unit in range(2):
         pl.when(x != c + 2 * unit)(lambda: x_copy(unit).wait_send())
     run("sides")

time: 78.9 us -> 76.5 us (0.970)
  Pallas kernels: 76.2 us -> 74.1 us
    pallas_call x1, Pallas kernels: 76.2 us -> 74.1 us  [local(): pl.pallas_call(body, out_shape=jax.ShapeDtypeStruct((32, 2048), BF16), in...]
where the time goes in v6:
time: 76.5 us; the launch traced here: 75.7 us
  Pallas kernels  74.1 us (97%)
  local copies, waits for them, and re-layouts  1.57 us (2%)
    pallas_call x1, Pallas kernels, local(): pl.pallas_call(body, out_shape=jax.ShapeDtypeStruct((32, 2048), BF16), in...  74.1 us
    unnamed x1, local copies, waits for them, and re-layouts  1.57 us

profile of v6, /device:TPU:0, one launch (start us, length us, event | category | flops | bytes accessed | tf_op | source)
XLA Modules:
  0.0 75.7 jit_solution(1437573447594586931)
XLA Ops:
  0.0 74.1 %shard_map.136 = bf16[32,2048]{1,0:T(8,128)(2,1)} custom-call(bf16[256,128]{1,0:T(8,128)(2,1)} %qn_hbm.1, bf16[256,128]{1,0:T(8,128)(2,1)} %kn_hbm.1, bf16[256,128]{1,0:T(8,128)(2,1)} %vn_hbm.1, bf16[256,128]{1,0:T(8,128)(2,1)} %qb_hbm.1, bf16[256,128]{1,0:T(8,128)(2,1)} %kb_hbm.1, bf16[256,128]{1,0:T(8,128)(2,1)} %vb_hbm.1, bf16[2,256]{1,0:T(2,128)(2,1)} %offn_ref.1, ...), custom_call_target="tpu_custom_call" | custom-call | tf_op jit(solution)/shard_map/pallas_call | solution.py:666
  74.1 1.6 %copy.16 = bf16[32,2048]{1,0:T(8,128)(2,1)} copy(bf16[32,2048]{1,0:T(8,128)(2,1)} %shard_map.136) | data formatting | bytes 262144

commit v7 on v6

--- a/solution.py
+++ b/solution.py
@@ -258,7 +258,7 @@
 
     def send(g, slot, q, axis, step, dx, dz):
         ref = piece(g, slot, q)
-        remote(ref, ref, send_sem.at[g], recv_sem.at[g, q, dz * 4 + dx], neighbour[axis, step]).start()
+        remote(ref, ref, send_sem.at[g], recv_sem.at[g, q, dz * 4 + dx - 1], neighbour[axis, step]).start()
 
     def run(point):
         for kind, g, q, what in PLAN[point]:
@@ -268,7 +268,7 @@
                 send(g, xz(-here[0], -here[1]), q, axis, step, dx, dz)
             else:
                 dx, dz = what
-                arrived(piece(g, xz(-dx, -dz), q), recv_sem.at[g, q, dz * 4 + dx])
+                arrived(piece(g, xz(-dx, -dz), q), recv_sem.at[g, q, dz * 4 + dx - 1])
 
     arrived(head_buf, load_sem.at[0])
 
@@ -581,9 +581,10 @@
     def cols(r):
         return pl.ds(r * 512, 512)
 
-    def pair_copy(r):
+    def pair_copy(r, half):
+        columns = pl.ds(r * 512 + half * 256, 256)
         return remote(
-            part_buf.at[1 - c, :, :, cols(r)], pair_buf.at[:, :, cols(r)], y_send.at[0], pair_sem.at[r],
+            part_buf.at[1 - c, :, :, columns], pair_buf.at[:, :, columns], y_send.at[0], pair_sem.at[r],
             neighbour["pair"],
         )
 
@@ -604,7 +605,7 @@
         return part_buf[c, yy, :, cols(r)].astype(F32) + pair_buf[yy, :, cols(r)].astype(F32)
 
     def pair_step(r):
-        pair_copy(r).wait_recv()
+        arrived(pair_buf.at[:, :, cols(r)], pair_sem.at[r])
         for k, dy in enumerate((2, 1, -1)):
             last_out[k, :, cols(r)] = pair_sum(r, dy).astype(BF16)
             last_copy(r, k).start()
@@ -623,7 +624,7 @@
             w = jnp.concatenate([down_buf[slot], down_buf[slot + 1]], axis=1)
             value = jnp.dot(hidden_buf[...], w, preferred_element_type=F32)
             store_part(value, pl.ds(r * 512 + pair * 256, 256), 256)
-        pair_copy(r).start()
+            pair_copy(r, pair).start()
 
     def finish(r, dz):
         columns = pl.ds(pl.multiple_of(lax.rem(z - dz + 4, 4) * 512, 512), 512)
@@ -695,7 +696,7 @@
             pltpu.VMEM((256, 1024), BF16),
             pltpu.VMEM((32, 2048), BF16),
             dma((7,)),
-            dma((2, 4, 16)),
+            dma((2, 4, 15)),
             dma((2,)),
             dma((4,)),
             dma((2,)),

time: 76.5 us -> 76.9 us (level)
  no operation moved by 1% of the time
where the time goes in v7:
time: 76.9 us; the launch traced here: 76 us
  Pallas kernels  74.4 us (97%)
  local copies, waits for them, and re-layouts  1.57 us (2%)
    pallas_call x1, Pallas kernels, local(): pl.pallas_call(body, out_shape=jax.ShapeDtypeStruct((32, 2048), BF16), in...  74.4 us
    unnamed x1, local copies, waits for them, and re-layouts  1.57 us

profile of v7, /device:TPU:0, one launch (start us, length us, event | category | flops | bytes accessed | tf_op | source)
XLA Modules:
  0.0 76.0 jit_solution(5768735298258855343)
XLA Ops:
  0.0 74.4 %shard_map.136 = bf16[32,2048]{1,0:T(8,128)(2,1)} custom-call(bf16[256,128]{1,0:T(8,128)(2,1)} %qn_hbm.1, bf16[256,128]{1,0:T(8,128)(2,1)} %kn_hbm.1, bf16[256,128]{1,0:T(8,128)(2,1)} %vn_hbm.1, bf16[256,128]{1,0:T(8,128)(2,1)} %qb_hbm.1, bf16[256,128]{1,0:T(8,128)(2,1)} %kb_hbm.1, bf16[256,128]{1,0:T(8,128)(2,1)} %vb_hbm.1, bf16[2,256]{1,0:T(2,128)(2,1)} %offn_ref.1, ...), custom_call_target="tpu_custom_call" | custom-call | tf_op jit(solution)/shard_map/pallas_call | solution.py:667
  74.4 1.6 %copy.16 = bf16[32,2048]{1,0:T(8,128)(2,1)} copy(bf16[32,2048]{1,0:T(8,128)(2,1)} %shard_map.136) | data formatting | bytes 262144

commit v8 on v6

--- a/solution.py
+++ b/solution.py
@@ -258,7 +258,7 @@
 
     def send(g, slot, q, axis, step, dx, dz):
         ref = piece(g, slot, q)
-        remote(ref, ref, send_sem.at[g], recv_sem.at[g, q, dz * 4 + dx], neighbour[axis, step]).start()
+        remote(ref, ref, send_sem.at[g], recv_sem.at[g, q, dz * 4 + dx - 1], neighbour[axis, step]).start()
 
     def run(point):
         for kind, g, q, what in PLAN[point]:
@@ -268,7 +268,7 @@
                 send(g, xz(-here[0], -here[1]), q, axis, step, dx, dz)
             else:
                 dx, dz = what
-                arrived(piece(g, xz(-dx, -dz), q), recv_sem.at[g, q, dz * 4 + dx])
+                arrived(piece(g, xz(-dx, -dz), q), recv_sem.at[g, q, dz * 4 + dx - 1])
 
     arrived(head_buf, load_sem.at[0])
 
@@ -695,7 +695,7 @@
             pltpu.VMEM((256, 1024), BF16),
             pltpu.VMEM((32, 2048), BF16),
             dma((7,)),
-            dma((2, 4, 16)),
+            dma((2, 4, 15)),
             dma((2,)),
             dma((4,)),
             dma((2,)),

time: 76.5 us -> 76.5 us (level)
  no operation moved by 1% of the time
where the time goes in v8:
time: 76.5 us; the launch traced here: 75.6 us
  Pallas kernels  74 us (97%)
  local copies, waits for them, and re-layouts  1.57 us (2%)
    pallas_call x1, Pallas kernels, local(): pl.pallas_call(body, out_shape=jax.ShapeDtypeStruct((32, 2048), BF16), in...  74 us
    unnamed x1, local copies, waits for them, and re-layouts  1.57 us

profile of v8, /device:TPU:0, one launch (start us, length us, event | category | flops | bytes accessed | tf_op | source)
XLA Modules:
  0.0 75.6 jit_solution(438305010792086965)
XLA Ops:
  0.0 74.0 %shard_map.136 = bf16[32,2048]{1,0:T(8,128)(2,1)} custom-call(bf16[256,128]{1,0:T(8,128)(2,1)} %qn_hbm.1, bf16[256,128]{1,0:T(8,128)(2,1)} %kn_hbm.1, bf16[256,128]{1,0:T(8,128)(2,1)} %vn_hbm.1, bf16[256,128]{1,0:T(8,128)(2,1)} %qb_hbm.1, bf16[256,128]{1,0:T(8,128)(2,1)} %kb_hbm.1, bf16[256,128]{1,0:T(8,128)(2,1)} %vb_hbm.1, bf16[2,256]{1,0:T(2,128)(2,1)} %offn_ref.1, ...), custom_call_target="tpu_custom_call" | custom-call | tf_op jit(solution)/shard_map/pallas_call | solution.py:666
  74.0 1.6 %copy.16 = bf16[32,2048]{1,0:T(8,128)(2,1)} copy(bf16[32,2048]{1,0:T(8,128)(2,1)} %shard_map.136) | data formatting | bytes 262144
